TPU v7x, 256 devices: a whole 4x4x8 slice. The times are simulated.
256 devices in a mesh: ep: 64 (over z, y, core), tp: 4 (over x).
Axes of the slice: x: 4, y: 4, z: 8, core: 2. Of those that a mesh axis runs over, the one named last changes fastest.
Arguments:
- glu_value: bfloat16 [32768, 1024], P('ep', 'tp'), may hold values from -6 to 6
- glu_gate: bfloat16 [32768, 1024], P('ep', 'tp'), may hold values from -12 to 12
- conv_kernel: float32 [31, 1024], P(None, 'tp'), may hold values from -11.49474 to 11.49474
- ln_gain: float32 [1024], P('tp'), may hold values from 0.1 to 1.9
- out_weight: bfloat16 [1024, 2048], P('tp'), may hold values from -0.1875 to 0.1875
- moe_input: bfloat16 [16384, 2048], P('ep'), may hold values from -6 to 6
- moe_gain: float32 [2048], replicated, may hold values from 0.1 to 1.9
- gate_weight: bfloat16 [64, 2048, 3072], P('ep', None, 'tp'), may hold values from -0.125 to 0.125
- up_weight: bfloat16 [64, 2048, 3072], P('ep', None, 'tp'), may hold values from -0.125 to 0.125
- down_weight: bfloat16 [64, 3072, 2048], P('ep', 'tp'), may hold values from -0.109375 to 0.109375
- expert_ids: int32 [16384, 2], P('ep'), may hold values from 0 to 63, all different within a row; in each aligned block of 256 rows (0 to 255, 256 to 511, ...) at most 16 rows name the same one
- route_weight: float32 [16384, 2], P('ep'), may hold values from 0.2 to 1
Outputs:
- mixer_out: bfloat16 [32768, 2048], P(('ep', 'tp'))
- expert_out: bfloat16 [16384, 2048], P('ep', 'tp')
Inputs may be any that keep to these rules, and one draw needn't show every extreme that they name: `expert_ids`: each row names 2 different experts. In the rows of one device no expert is named by more than 16 rows; the bound is reached at some expert in some device's rows.
All inputs are finite; a program needn't handle non-finite values.
Results may differ from a plain program's by a relative error of at most 0.012.
Values may be sent and summed in bfloat16 or wider, within the bound.
No kernel may reach another device: no remote copies, remote signals or barrier semaphores. Data moves between devices by JAX's collectives and lax.ppermute only.
A program may use at most 64 MiB of HBM per device.

v0:
```python
import jax
import jax.numpy as jnp
from jax import lax
from jax.sharding import PartitionSpec as P

eps_rms = 1e-06
eps_norm = 1e-05


def from_behind(value, axis, by):
    count = lax.axis_size(axis)
    pairs = [(i, i + by) for i in range(count) if 0 <= i + by < count]
    return lax.ppermute(value, axis, pairs)


def slot_numbers(expert_ids, experts, capacity):
    chosen = expert_ids.reshape(-1)
    onehot = (chosen[:, None] == jnp.arange(experts, dtype=jnp.int32)[None, :]).astype(jnp.int32)
    earlier = jnp.cumsum(onehot, axis=0) - onehot
    position = jnp.sum(earlier * onehot, axis=1)
    return chosen * capacity + position


def fill_slots(normed, slot_index, experts, capacity, chosen_per_token):
    owners = jnp.full((experts * capacity,), -1, jnp.int32)
    token_of = jnp.arange(slot_index.shape[0], dtype=jnp.int32) // chosen_per_token
    owners = owners.at[slot_index].set(token_of)
    picked = jnp.take(normed, jnp.maximum(owners, 0), axis=0)
    filled = jnp.where((owners >= 0)[:, None], picked, jnp.zeros_like(picked))
    return filled.reshape(experts, capacity, normed.shape[1])


def on_device(
    glu_value,
    glu_gate,
    conv_kernel,
    ln_gain,
    out_weight,
    moe_input,
    moe_gain,
    gate_weight,
    up_weight,
    down_weight,
    expert_ids,
    route_weight,
):
    length, channels_dev = glu_value.shape
    reach = conv_kernel.shape[0]
    tp_count = lax.axis_size("tp")
    gated = (glu_value.astype(jnp.float32) * jax.nn.sigmoid(glu_gate.astype(jnp.float32))).astype(
        jnp.bfloat16
    )
    earlier_rows = from_behind(gated[length - (reach - 1) :], "ep", 1)
    padded = jnp.concatenate([earlier_rows, gated], axis=0).astype(jnp.float32)
    convolved = jnp.zeros((length, channels_dev), jnp.float32)
    for tap_index in range(reach):
        begin = reach - 1 - tap_index
        convolved = convolved + conv_kernel[tap_index] * padded[begin : begin + length]
    total, squares = lax.psum(
        (jnp.sum(convolved, axis=1), jnp.sum(convolved * convolved, axis=1)), "tp"
    )
    channels = channels_dev * tp_count
    mean = total / channels
    variance = squares / channels - mean * mean
    scaled = (convolved - mean[:, None]) * lax.rsqrt(variance + eps_norm)[:, None] * ln_gain
    activated = jax.nn.silu(scaled).astype(jnp.bfloat16)
    mixer_out = lax.psum_scatter(
        jnp.dot(activated, out_weight, preferred_element_type=jnp.float32).astype(jnp.bfloat16),
        "tp",
        scatter_dimension=0,
        tiled=True,
    )
    tokens, model_width = moe_input.shape
    chosen_per_token = expert_ids.shape[1]
    experts = lax.axis_size("ep")
    capacity = 4 * max(1, tokens // experts)
    values = moe_input.astype(jnp.float32)
    normed = (
        values * lax.rsqrt(jnp.mean(values * values, axis=1, keepdims=True) + eps_rms) * moe_gain
    ).astype(jnp.bfloat16)
    slot_index = slot_numbers(expert_ids, experts, capacity)
    outgoing = fill_slots(normed, slot_index, experts, capacity, chosen_per_token)
    w_gate = gate_weight[0]
    w_up = up_weight[0]
    w_down = down_weight[0]
    quarter_slots = capacity // tp_count
    own_slots = lax.dynamic_slice_in_dim(
        outgoing, lax.axis_index("tp") * quarter_slots, quarter_slots, 1
    )
    arrived_part = lax.all_to_all(own_slots, "ep", split_axis=0, concat_axis=0, tiled=True)
    arrived = lax.all_gather(arrived_part, "tp", axis=1, tiled=True)
    flattened = arrived.reshape(-1, model_width)
    gate_act = jnp.dot(flattened, w_gate, preferred_element_type=jnp.float32)
    up_act = jnp.dot(flattened, w_up, preferred_element_type=jnp.float32)
    hidden_rows = (jax.nn.silu(gate_act) * up_act).astype(jnp.bfloat16)
    hidden = hidden_rows.reshape(arrived.shape[0], arrived.shape[1], w_gate.shape[1])
    sources = hidden.shape[0]
    partial_sum = jnp.dot(
        hidden.reshape(-1, hidden.shape[2]), w_down, preferred_element_type=jnp.float32
    )
    partial_sum = partial_sum.reshape(sources, capacity, model_width)
    answers = lax.psum_scatter(
        partial_sum.astype(jnp.bfloat16), "tp", scatter_dimension=2, tiled=True
    )
    returned = lax.all_to_all(answers, "ep", split_axis=0, concat_axis=0, tiled=True)
    feature_dev = returned.shape[2]
    picked = jnp.take(returned.reshape(experts * capacity, feature_dev), slot_index, axis=0)
    picked = picked.astype(jnp.float32).reshape(tokens, chosen_per_token, feature_dev)
    expert_out = jnp.sum(picked * route_weight[:, :, None], axis=1).astype(jnp.bfloat16)
    return (mixer_out, expert_out)


def solution(mesh):
    in_specs = (
        P("ep", "tp"),
        P("ep", "tp"),
        P(None, "tp"),
        P("tp"),
        P("tp", None),
        P("ep", None),
        P(),
        P("ep", None, "tp"),
        P("ep", None, "tp"),
        P("ep", "tp", None),
        P("ep", None),
        P("ep", None),
    )
    out_specs = (P(("ep", "tp"), None), P("ep", "tp"))
    return jax.shard_map(
        on_device, mesh=mesh, in_specs=in_specs, out_specs=out_specs, check_vma=False
    )
```

profile of v0, /device:TPU:1, one launch (start us, length us, event | category | flops | bytes accessed | tf_op | source)
XLA Modules:
  0.0 243.3 jit_solution(11828817897513829075)
XLA Ops:
  7.2 0.0 all-gather.2.cloned.1.call-start
  7.2 1.0 copy.45
  8.2 0.1 eq.26
  8.3 0.1 reshape.105
  8.5 0.7 broadcast_multiply_fusion
  9.2 1.2 reduce-window.6
  10.4 0.2 slice_reduce_fusion
  10.7 0.1 copy.50
  10.8 0.1 mul.502
  11.0 0.1 fusion.47
  11.1 2.4 %scatter_custom_fusion = s32[1024]{0:T(1024)S(1)} fusion(s32[512]{0:T(512)S(1)} %bitcast.76, s32[512]{0:T(512)S(1)} %add_select_fusion, s32[]{:T(128)} %constant.76.clone.1), kind=kCustom, calls=%fused_computation.111 | custom fusion | bytes 4100 | tf_op jit(solution)/shard_map/scatter | solution.py:27
  13.6 0.1 broadcast_in_dim.51
  13.7 0.1 broadcast_in_dim.53
  13.8 1.5 fusion.7
  15.3 2.5 %fusion.9 = bf16[256,2048]{1,0:T(8,128)(2,1)} fusion(bf16[256,2048]{1,0:T(8,128)(2,1)} %param.17, f32[2048]{0:T(1024)} %param.18, f32[256]{0:T(256)S(1)} %add_rsqrt_fusion.1), kind=kLoop, calls=%fused_computation.15 | loop fusion | flops 2097152 | bytes 2106368 | tf_op jit(solution)/shard_map/convert_element_type | solution.py:80
  17.8 10.2 %gather_fusion = bf16[1024,2048]{1,0:T(8,128)(2,1)} fusion(bf16[256,2048]{1,0:T(8,128)(2,1)} %fusion.9, s32[1024]{0:T(1024)S(1)} %maximum_clamp_fusion), kind=kCustom, calls=%fused_computation | custom fusion | bytes 8392704 | tf_op jit(solution)/shard_map/jit(_take)/gather | solution.py:28
  28.0 0.1 constant_dynamic-slice_fusion
  28.1 2.5 %fusion.10 = bf16[64,4,2048]{2,1,0:T(4,128)(2,1)S(1)} fusion(bf16[64,16,2048]{2,1,0:T(8,128)(2,1)} %bitcast.72, s32[]{:T(128)S(6)} %select_n.48, pred[64,4]{1,0:T(8,128)(4,1)S(1)} %get-tuple-element.43, pred[64,4]{1,0:T(8,128)(4,1)S(1)} %get-tuple-element.42), kind=kLoop, calls=%fused_computation.17 | loop fusion | flops 1048576 | bytes 2097668 | tf_op jit(solution)/shard_map/jit(_where)/select_n | solution.py:29
  30.6 41.1 %all_to_all.10 = bf16[64,4,2048]{2,1,0:T(4,128)(2,1)S(1)} all-to-all(bf16[64,4,2048]{2,1,0:T(4,128)(2,1)S(1)} %fusion.10), channel_id=1, replica_groups=mesh['ep'=64,'tp'=4] {'ep'}, dimensions={0} | all-to-all | bytes 2097152 | tf_op jit(solution)/shard_map/all_to_all | solution.py:90
  71.7 1.6 copy.51
  73.2 0.0 all-gather.2.cloned.1.call-update
  73.3 0.2 reduce-scatter.5.cloned.1.call-start
  73.5 47.4 %all-gather.2.cloned.1.call-done = bf16[64,16,2048]{2,0,1:T(8,128)(2,1)} async-done(((bf16[64,4,2048]{2,0,1:T(8,128)(2,1)}), bf16[64,16,2048]{2,0,1:T(8,128)(2,1)}) %all-gather.2.cloned.1.call-update) | async-done | bytes 4194320 | tf_op jit(solution)/shard_map/all_gather | solution.py:91
  120.9 4.6 %copy.52 = bf16[64,16,2048]{2,1,0:T(8,128)(2,1)S(1)} copy(bf16[64,16,2048]{2,0,1:T(8,128)(2,1)} %all-gather.2.cloned.1.call-done) | data formatting | bytes 8388608 | tf_op jit(solution)/shard_map/all_gather | solution.py:91
  125.5 3.4 %fusion.1 = f32[1024,768]{1,0:T(8,128)S(1)} fusion(bf16[1024,2048]{1,0:T(8,128)(2,1)S(1)} %bitcast.73, bf16[1,2048,768]{2,1,0:T(8,128)(2,1)S(1)} %copy-done.5), kind=kOutput, calls=%fused_computation.5 | convolution fusion | flops 3221225472 | bytes 10485760 | tf_op jit(solution)/shard_map/dot_general | solution.py:94
  129.0 3.7 %multiply_convert_fusion = bf16[1024,768]{1,0:T(8,128)(2,1)S(1)} fusion(f32[1024,768]{1,0:T(8,128)S(1)} %fusion.1, bf16[1024,2048]{1,0:T(8,128)(2,1)S(1)} %bitcast.74, bf16[1,2048,768]{2,1,0:T(8,128)(2,1)S(1)} %copy-done.6), kind=kOutput, calls=%fused_computation.9 | convolution fusion | flops 3225944064 | bytes 12058624 | tf_op jit(solution)/shard_map/dot_general | solution.py:93
  132.7 5.0 %convolution_convert_fusion = bf16[64,16,2048]{2,1,0:T(8,128)(2,1)} fusion(bf16[64,16,768]{2,1,0:T(8,128)(2,1)S(1)} %bitcast.109, bf16[1,768,2048]{2,1,0:T(8,128)(2,1)S(1)} %copy-done), kind=kOutput, calls=%fused_computation.3 | convolution fusion | flops 3223322624 | bytes 8912896 | tf_op jit(solution)/shard_map/dot_general | solution.py:98
  137.7 0.0 reduce-scatter.5.cloned.1.call-update
  137.8 0.0 reduce-scatter.3.cloned.1.call-start
  137.8 0.9 copy-done.1
  138.7 1.1 multiply_convert_fusion.2
  139.8 3.8 %collective-permute-start = (bf16[30,256]{1,0:T(8,128)(2,1)S(1)}, bf16[30,256]{1,0:T(8,128)(2,1)S(1)}, u32[]{:S(2)}, u32[]{:S(2)}) collective-permute-start(bf16[30,256]{1,0:T(8,128)(2,1)S(1)} %slice.264), channel_id=1, source_target_pairs={{0,4},{4,8},{8,12},{12,16},{16,20},{20,24},{24,28},{28,32},{32,36}... | collective-permute-start | bytes 46088 | tf_op jit(solution)/shard_map/ppermute | solution.py:13
  143.7 0.8 collective-permute-done
  144.5 0.1 maximum_convert_fusion
  144.6 2.9 %fusion.55 = (f32[512]{0:T(512)S(1)}, f32[512]{0:T(512)S(1)}, f32[512,256]{1,0:T(8,128)}) fusion(f32[542,256]{1,0:T(8,128)S(1)} %maximum_convert_fusion, f32[256]{0:T(256)S(1)} %bitcast.107, f32[256]{0:T(256)S(1)} %bitcast.108, f32[256]{0:T(256)S(1)} %bitcast.79, f32[256]{0:T(256)S(1)} %bitcast.80, f32[256]{0:T(256)S(1)} %bitcast.81, f32[256]{0:T(256)S(1)} %bitcast.82, ...), kind=kLoop, calls=%fused_computation.121 | loop fusion | flops 8387584 | bytes 16813056 | tf_op jit(solution)/shard_map/reduce_sum | solution.py:60
  147.5 7.3 %all-reduce = (f32[512]{0:T(512)S(1)}, f32[512]{0:T(512)S(1)}) all-reduce(f32[512]{0:T(512)S(1)} %get-tuple-element.3, f32[512]{0:T(512)S(1)} %get-tuple-element.2), channel_id=1, replica_groups=mesh['ep'=64,'tp'=4] {'tp'}, use_global_device_ids=true, to_apply=%region_3.0 | all-reduce | flops 1024 | bytes 8192 | tf_op jit(solution)/shard_map/psum | solution.py:59
  154.8 3.5 %convolution_convert_fusion.1 = bf16[512,2048]{1,0:T(8,128)(2,1)} fusion(bf16[256,2048]{1,0:T(8,128)(2,1)} %param.16, f32[512,256]{1,0:T(8,128)} %get-tuple-element.6, f32[256]{0:T(256)S(1)} %copy-done.7, f32[512]{0:T(512)S(1)} %get-tuple-element.41, f32[512]{0:T(512)S(1)} %get-tuple-element.40), kind=kOutput, calls=%fused_computation.10 | convolution fusion | flops 538968064 | bytes 3675136 | tf_op jit(solution)/shard_map/dot_general | solution.py:68
  158.4 0.0 reduce-scatter.3.cloned.1.call-update
  158.4 29.4 %reduce-scatter.5.cloned.1.call-done = bf16[64,16,512]{2,1,0:T(8,128)(2,1)} async-done(((bf16[64,16,2048]{2,1,0:T(8,128)(2,1)}), bf16[64,16,512]{2,1,0:T(8,128)(2,1)}) %reduce-scatter.5.cloned.1.call-update) | async-done | bytes 1048592 | tf_op jit(solution)/shard_map/reduce_scatter | solution.py:102
  187.8 11.0 %all-to-all-start.1 = ((bf16[64,16,512]{2,1,0:T(8,128)(2,1)}), bf16[64,16,512]{2,1,0:T(8,128)(2,1)}, u32[]{:S(2)}, u32[]{:S(2)}) async-start(bf16[64,16,512]{2,1,0:T(8,128)(2,1)} %reduce-scatter.5.cloned.1.call-done), calls=%async_computation.3 | async-start | bytes 2097152 | tf_op jit(solution)/shard_map/all_to_all | solution.py:105
  198.8 0.1 reduce_sum.52
  199.0 0.1 copy.48
  199.1 0.2 copy.49
  199.3 0.1 copy.53
  199.4 27.5 %all-to-all-done.1 = bf16[64,16,512]{2,1,0:T(8,128)(2,1)} async-done(((bf16[64,16,512]{2,1,0:T(8,128)(2,1)}), bf16[64,16,512]{2,1,0:T(8,128)(2,1)}, u32[]{:S(2)}, u32[]{:S(2)}) %all-to-all-start.1) | async-done | bytes 1048608 | tf_op jit(solution)/shard_map/all_to_all | solution.py:105
  226.9 4.0 %gather_fusion.1 = bf16[512,512]{1,0:T(8,128)(2,1)} fusion(bf16[1024,512]{1,0:T(8,128)(2,1)} %bitcast.41, s32[1024]{0:T(1024)S(1)} %pad_clamp_fusion), kind=kCustom, calls=%fused_computation.1 | custom fusion | bytes 1050624 | tf_op jit(solution)/shard_map/jit(_take)/gather | solution.py:107
  230.9 2.0 gather.15
  232.9 3.9 %multiply_reduce_fusion = bf16[256,512]{1,0:T(8,128)(2,1)} fusion(bf16[256,2,512]{2,1,0:T(2,128)(2,1)} %gather.15, pred[256,2]{1,0:T(8,128)(4,1)S(1)} %copy.49, f32[256,2]{1,0:T(8,128)S(1)} %copy.53), kind=kLoop, calls=%fused_computation.18 | loop fusion | flops 917504 | bytes 788992 | tf_op jit(solution)/shard_map/reduce_sum | solution.py:109
  (30 shorter events, 0.2 us)
Async XLA Ops:
  7.2 125.6 %copy-start = (bf16[1,768,2048]{2,1,0:T(8,128)(2,1)S(1)}, bf16[1,768,2048]{2,1,0:T(8,128)(2,1)}, u32[]{:S(2)}) copy-start(bf16[1,768,2048]{2,1,0:T(8,128)(2,1)} %param.21) | copy-start | bytes 9437188
  7.2 113.7 %all-gather.2.cloned.1.call-start = ((), (), s32[]{:S(2)}) async-start(), calls=%async_computation.5 | async-start | bytes 5242880 | tf_op jit(solution)/shard_map/all_gather | solution.py:91
  73.3 114.6 %reduce-scatter.5.cloned.1.call-start = ((), (), s32[]{:S(2)}) async-start(), calls=%async_computation.6 | async-start | bytes 5242880 | tf_op jit(solution)/shard_map/reduce_scatter | solution.py:102
  120.9 4.6 %copy-start.5 = (bf16[1,2048,768]{2,1,0:T(8,128)(2,1)S(1)}, bf16[1,2048,768]{2,1,0:T(8,128)(2,1)}, u32[]{:S(2)}) copy-start(bf16[1,2048,768]{2,1,0:T(8,128)(2,1)} %param.20) | copy-start | bytes 9437188
  125.5 3.5 %copy-start.6 = (bf16[1,2048,768]{2,1,0:T(8,128)(2,1)S(1)}, bf16[1,2048,768]{2,1,0:T(8,128)(2,1)}, u32[]{:S(2)}) copy-start(bf16[1,2048,768]{2,1,0:T(8,128)(2,1)} %param.19) | copy-start | bytes 9437188
  137.7 0.9 copy-start.1
  137.7 5.9 %copy-start.2 = (f32[31,256]{1,0:T(8,128)S(1)}, f32[31,256]{1,0:T(8,128)}, u32[]{:S(2)}) copy-start(f32[31,256]{1,0:T(8,128)} %param.14) | copy-start | bytes 95236
  137.8 99.1 %reduce-scatter.3.cloned.1.call-start = ((), (), s32[]{:S(2)}) async-start(), calls=%async_computation.4 | async-start | bytes 2621440 | tf_op jit(solution)/shard_map/reduce_scatter | solution.py:67
  139.8 4.7 %collective-permute-start = (bf16[30,256]{1,0:T(8,128)(2,1)S(1)}, bf16[30,256]{1,0:T(8,128)(2,1)S(1)}, u32[]{:S(2)}, u32[]{:S(2)}) collective-permute-start(bf16[30,256]{1,0:T(8,128)(2,1)S(1)} %slice.264), channel_id=1, source_target_pairs={{0,4},{4,8},{8,12},{12,16},{16,20},{20,24},{24,28},{28,32},{32,36}... | collective-permute-start | bytes 46088 | tf_op jit(solution)/shard_map/ppermute | solution.py:13
  144.5 10.3 %copy-start.7 = (f32[256]{0:T(256)S(1)}, f32[256]{0:T(256)}, u32[]{:S(2)}) copy-start(f32[256]{0:T(256)} %param.15) | copy-start | bytes 3076
  158.4 40.7 %copy-start.3 = (s32[256,2]{0,1:T(2,128)S(1)}, s32[256,2]{0,1:T(2,128)}, u32[]{:S(2)}) copy-start(s32[256,2]{0,1:T(2,128)} %param.22) | copy-start | bytes 6148
  158.4 40.9 %copy-start.4 = (f32[256,2]{0,1:T(2,128)S(1)}, f32[256,2]{0,1:T(2,128)}, u32[]{:S(2)}) copy-start(f32[256,2]{0,1:T(2,128)} %param.23) | copy-start | bytes 6148
  187.8 39.1 %all-to-all-start.1 = ((bf16[64,16,512]{2,1,0:T(8,128)(2,1)}), bf16[64,16,512]{2,1,0:T(8,128)(2,1)}, u32[]{:S(2)}, u32[]{:S(2)}) async-start(bf16[64,16,512]{2,1,0:T(8,128)(2,1)} %reduce-scatter.5.cloned.1.call-done), calls=%async_computation.3 | async-start | bytes 2097152 | tf_op jit(solution)/shard_map/all_to_all | solution.py:105
Sparse Core Ops, SparseCore 0:
  73.4 47.4 all-gather.1
  137.9 49.9 reduce-scatter.4
  191.0 31.9 reduce-scatter.2
where the time goes:
time: 244 us; the launch traced here: 243 us
  waiting for transfers between devices  105 us (43%)
  blocking collectives  48.5 us (20%)
  local copies, waits for them, and re-layouts  28.4 us (12%)
  other arithmetic  16.6 us (7%)
  matrix products  15.7 us (6%)
  starting transfers between devices  15.1 us (6%)
  between operations  14 us (6%)
    all_gather x1, waiting for transfers between devices, on_device(): arrived = lax.all_gather(arrived_part, 'tp', axis=1, tiled=True)  47.4 us
    all_to_all x1, blocking collectives, on_device(): lax.all_to_all(own_slots, 'ep', split_axis=0, concat_axis=0, tiled=True)  41.1 us
    reduce_scatter x1, waiting for transfers between devices, on_device(): lax.psum_scatter(partial_sum.astype(jnp.bfloat16), 'tp', scatter_dimensio...  29.4 us
    all_to_all x1, waiting for transfers between devices, on_device(): lax.all_to_all(answers, 'ep', split_axis=0, concat_axis=0, tiled=True)  27.5 us
    all_to_all x1, starting transfers between devices, on_device(): lax.all_to_all(answers, 'ep', split_axis=0, concat_axis=0, tiled=True)  11 us
    gather x1, local copies, waits for them, and re-layouts, fill_slots(): picked = jnp.take(normed, jnp.maximum(owners, 0), axis=0)  10.2 us
    psum x1, blocking collectives, on_device(): lax.psum((jnp.sum(convolved, axis=1), jnp.sum(convolved * convolved, axis...  7.35 us
    gather x2, local copies, waits for them, and re-layouts, on_device(): jnp.take(returned.reshape(experts * capacity, feature_dev), slot_index, a...  6.05 us
  transfers between devices with their start and end apart: 5, of which 4 were waited for; matrix products, arithmetic and copies ran while one was open for 7% of the time, Pallas kernels for 0%

commit v1 on v0

v1 whole, which is shorter than its diff:
```python
import functools

import jax
import jax.numpy as jnp
from jax import lax
from jax.experimental import pallas as pl
from jax.experimental.pallas import tpu as pltpu
from jax.sharding import PartitionSpec as P


eps_rms = 1e-06
eps_norm = 1e-05
f32 = jnp.float32
bf16 = jnp.bfloat16


VMEM = pl.BlockSpec(memory_space=pltpu.VMEM)
SMEM = pl.BlockSpec(memory_space=pltpu.SMEM)
ANY = pl.BlockSpec(memory_space=pl.ANY)


def dot(a, b):
    return jnp.dot(a, b, preferred_element_type=f32)


def over_tp(value, by):
    count = lax.axis_size("tp")
    return lax.ppermute(value, "tp", [(i, (i + by) % count) for i in range(count)])


def from_behind(value, axis, by):
    count = lax.axis_size(axis)
    return lax.ppermute(value, axis, [(i, i + by) for i in range(count - by)])


def swap_cores(value):
    count = lax.axis_size("ep")
    return lax.ppermute(value, "ep", [(i, i ^ 1) for i in range(count)])


def gather_direct(value):
    return over_tp(value, -1), over_tp(value, 1), over_tp(value, 2)


def gather_relayed(value):
    half = value.shape[0] // 2
    ahead = over_tp(value, -1)
    behind = over_tp(value, 1)
    top = over_tp(ahead[:half], -1)
    bottom = over_tp(behind[half:], 1)
    return ahead, behind, top, bottom


def slot_tables(ids, rows, tokens, per_chunk):
    expert_of = lax.broadcasted_iota(jnp.int32, (rows, tokens), 0) // per_chunk
    first = expert_of == ids[0:1, :]
    second = expert_of == ids[1:2, :]
    chosen = jnp.logical_or(first, second)
    before = (
        lax.broadcasted_iota(jnp.int32, (tokens, tokens), 0)
        < lax.broadcasted_iota(jnp.int32, (tokens, tokens), 1)
    ).astype(f32).astype(bf16)
    earlier = dot(chosen.astype(f32).astype(bf16), before).astype(jnp.int32)
    place = lax.broadcasted_iota(jnp.int32, (rows, tokens), 0) % per_chunk
    return first, second, chosen, earlier, place


def fetch(sources, targets, sems):
    copies = [
        pltpu.make_async_copy(source, target, sems.at[i])
        for i, (source, target) in enumerate(zip(sources, targets))
    ]
    for copy in copies:
        copy.start()
    return copies


def dispatch_kernel(per_chunk, tp_ref, x_hbm, gain_hbm, ids_hbm, o0, o1, x_ref, gain_ref, ids_ref, sems):
    outs = (o0, o1)
    tokens, width = x_ref.shape
    rows, part = o0.shape
    for copy in fetch((x_hbm, gain_hbm, ids_hbm), (x_ref, gain_ref, ids_ref), sems):
        copy.wait()
    squares = jnp.zeros((tokens, 128), f32)
    for begin in range(0, width, 128):
        block = x_ref[:, begin : begin + 128].astype(f32)
        squares = squares + block * block
    scale = lax.rsqrt(jnp.sum(squares, axis=1, keepdims=True) / width + eps_rms)
    start = pl.multiple_of(tp_ref[0] * part, part)
    mine = x_ref[:, pl.ds(start, part)].astype(f32)
    normed = (mine * scale * gain_ref[:, pl.ds(start, part)]).astype(bf16)
    _, _, chosen, earlier, place = slot_tables(ids_ref[...], rows, tokens, per_chunk)
    for chunk, out in enumerate(outs):
        pick = jnp.logical_and(chosen, earlier == place + chunk * per_chunk)
        out[...] = dot(pick.astype(f32).astype(bf16), normed).astype(bf16)


def route_kernel(per_chunk, ids_ref, weight_ref, high_ref, low_ref):
    tokens, slots = high_ref.shape
    rows = slots // 2
    first, second, _, earlier, place = slot_tables(ids_ref[...], rows, tokens, per_chunk)
    amount = jnp.where(first, weight_ref[0:1, :], jnp.where(second, weight_ref[1:2, :], 0.0))
    for chunk in range(2):
        weights = jnp.where(earlier == place + chunk * per_chunk, amount, 0.0).T
        high = weights.astype(bf16)
        high_ref[:, chunk * rows : (chunk + 1) * rows] = high
        low_ref[:, chunk * rows : (chunk + 1) * rows] = (weights - high.astype(f32)).astype(bf16)


def expert_kernel(chunk, tp_ref, own, ahead, behind, *refs):
    if chunk == 0:
        across_in, *refs = refs
    else:
        top, bottom, *refs = refs
    weights, outs, scratch = refs[:3], refs[3:-7], refs[-7:]
    kept, (to_ahead, to_behind, across), sems = scratch[:3], scratch[3:6], scratch[6]
    rows, part = own.shape
    half = rows // 2
    width = weights[0].shape[0]
    count = width // part
    tp = tp_ref[0]
    starts = [
        pl.multiple_of(lax.rem(tp + k, count) * part, part) for k in (0, 1, count - 1, 2)
    ]
    gate_ref, up_ref, down_ref = kept
    sources, targets = [], []
    for start in starts:
        for source, target in zip(weights[:2], kept[:2]):
            sources.append(source.at[pl.ds(start, part), :])
            targets.append(target.at[pl.ds(start, part), :])
    copies = fetch(sources + [weights[2]], targets + [down_ref], sems)
    if chunk == 0:
        to_own, ahead_out, behind_out, across_top, across_bottom = outs
        to_ahead, to_behind = ahead_out, behind_out
        blocks = (own, ahead, behind, across_in)
    else:
        to_own, ahead_top, ahead_bottom, behind_top, behind_bottom, across_top, across_bottom = outs
        across[:half, :] = top[...]
        across[half:, :] = bottom[...]
        blocks = (own, ahead, behind, across)

    def step(i, carry):
        at = pl.ds(pl.multiple_of(i * half, half), half)
        gate = None
        up = None
        for k, (x, start) in enumerate(zip(blocks, starts)):

            @pl.when(i == 0)
            def _():
                copies[2 * k].wait()
                copies[2 * k + 1].wait()

            block = x[at, :]
            g = dot(block, gate_ref[pl.ds(start, part), :])
            u = dot(block, up_ref[pl.ds(start, part), :])
            gate = g if gate is None else gate + g
            up = u if up is None else up + u
        hidden = (jax.nn.silu(gate) * up).astype(bf16)

        @pl.when(i == 0)
        def _():
            copies[-1].wait()

        for out, start in zip((to_own, to_ahead, to_behind, across), starts):
            out[at, :] = dot(hidden, down_ref[:, pl.ds(start, part)]).astype(bf16)
        return carry

    lax.fori_loop(0, 2, step, 0)
    across_top[...] = across[:half, :]
    across_bottom[...] = across[half:, :]
    if chunk == 1:
        ahead_top[...] = to_ahead[:half, :]
        ahead_bottom[...] = to_ahead[half:, :]
        behind_top[...] = to_behind[:half, :]
        behind_bottom[...] = to_behind[half:, :]


def fold_whole_kernel(ahead, top, behind, bottom, ahead_out, behind_out):
    half = top.shape[0]
    ahead_out[:half, :] = (ahead[:half, :].astype(f32) + top[...].astype(f32)).astype(bf16)
    ahead_out[half:, :] = ahead[half:, :]
    behind_out[:half, :] = behind[:half, :]
    behind_out[half:, :] = (behind[half:, :].astype(f32) + bottom[...].astype(f32)).astype(bf16)


def total_whole_kernel(own, first, second, out):
    out[...] = (own[...].astype(f32) + first[...].astype(f32) + second[...].astype(f32)).astype(bf16)


def fold_kernel(a, b, c, d, ab, cd):
    ab[...] = (a[...].astype(f32) + b[...].astype(f32)).astype(bf16)
    cd[...] = (c[...].astype(f32) + d[...].astype(f32)).astype(bf16)


def total_kernel(own, top0, top1, bottom0, bottom1, out):
    half = top0.shape[0]
    out[:half, :] = (
        own[:half, :].astype(f32) + top0[...].astype(f32) + top1[...].astype(f32)
    ).astype(bf16)
    out[half:, :] = (
        own[half:, :].astype(f32) + bottom0[...].astype(f32) + bottom1[...].astype(f32)
    ).astype(bf16)


def conv_kernel_body(reach, halo, b0, b1, b2, b3, out_ref, wide, kept):
    own = out_ref.shape[0]
    part = b0.shape[1]
    channels = 4 * part
    total = jnp.zeros((own, 128), f32)
    square = jnp.zeros((own, 128), f32)
    rows = own + halo
    gains = []
    for k, block in enumerate((b0, b1, b2, b3)):
        taps = sum(
            block[rows + i * (reach + 1) : rows + (i + 1) * (reach + 1), :].astype(f32)
            for i in range(3)
        )
        gains.append(taps[reach : reach + 1, :])
        for begin in range(0, part, 128):
            lanes = slice(begin, begin + 128)
            wide[...] = block[:rows, lanes].astype(f32)
            value = jnp.zeros((own, 128), f32)
            for j in range(reach):
                value = value + taps[j : j + 1, lanes] * wide[halo - j : halo - j + own, :]
            kept[:, k * part + begin : k * part + begin + 128] = value
            total = total + value
            square = square + value * value
    mean = jnp.sum(total, axis=1, keepdims=True) / channels
    variance = jnp.sum(square, axis=1, keepdims=True) / channels - mean * mean
    scale = lax.rsqrt(variance + eps_norm)
    for k in range(4):
        lanes = slice(k * part, (k + 1) * part)
        scaled = (kept[:, lanes] - mean) * scale * gains[k]
        out_ref[:, lanes] = jax.nn.silu(scaled).astype(bf16)


def mix_kernel(core_ref, act, own, n1, n2, n3, far_ref, out_ref):
    part = own.shape[0]
    columns = n1.shape[1]
    core = core_ref[0]
    near_at = pl.ds(pl.multiple_of(core * columns, columns), columns)
    far_at = pl.ds(pl.multiple_of((1 - core) * columns, columns), columns)
    cut = lambda k: act[:, k * part : (k + 1) * part]
    near = dot(cut(0), own[:, near_at]) + dot(cut(1), n1[...])
    near = near + dot(cut(2), n2[...]) + dot(cut(3), n3[...])
    out_ref[:, near_at] = near.astype(bf16)
    far = dot(cut(0), own[:, far_at]) + dot(act[:, part:], far_ref[...])
    out_ref[:, far_at] = far.astype(bf16)


def combine_kernel(high_ref, low_ref, a0_hbm, a1_hbm, out_ref, a0, a1, sems):
    rows = a0.shape[0]
    copies = fetch((a0_hbm, a1_hbm), (a0, a1), sems)
    total = None
    for chunk, (copy, answers) in enumerate(zip(copies, (a0, a1))):
        copy.wait()
        cols = slice(chunk * rows, (chunk + 1) * rows)
        for weights in (high_ref, low_ref):
            term = dot(weights[:, cols], answers[...])
            total = term if total is None else total + term
    out_ref[...] = total.astype(bf16)


def call(kernel, out_shape, in_specs, flops, limit, scratch=()):
    many = isinstance(out_shape, (list, tuple))
    return pl.pallas_call(
        kernel,
        out_shape=out_shape,
        in_specs=in_specs,
        out_specs=[VMEM] * len(out_shape) if many else VMEM,
        scratch_shapes=scratch,
        compiler_params=pltpu.CompilerParams(vmem_limit_bytes=limit * 1024 * 1024),
        cost_estimate=pl.CostEstimate(flops=flops, bytes_accessed=1 << 20, transcendentals=0),
    )


def shape(*dims):
    return jax.ShapeDtypeStruct(dims, bf16)


def split_three(value):
    high = value.astype(bf16)
    rest = value - high.astype(f32)
    middle = rest.astype(bf16)
    return high, middle, (rest - middle.astype(f32)).astype(bf16)


def mixer_half(glu_value, glu_gate, conv_kernel, ln_gain, out_weight):
    tp = lax.axis_index("tp")
    core = lax.axis_index("ep") % 2
    length, part = glu_value.shape
    reach = conv_kernel.shape[0]
    count = lax.axis_size("tp")
    own = length // count
    halo = 32
    columns = out_weight.shape[1] // 2
    mine = lax.dynamic_slice_in_dim(out_weight, core * columns, columns, 1)
    near = gather_direct(mine)
    far = swap_cores(jnp.concatenate(near, axis=0))
    taps = jnp.concatenate([conv_kernel, ln_gain[None, :]], axis=0)
    taps = split_three(taps)
    gated = (glu_value.astype(f32) * jax.nn.sigmoid(glu_gate.astype(f32))).astype(bf16)
    before = from_behind(gated[length - halo :], "ep", 1)
    padded = jnp.concatenate([before, gated], axis=0)

    def rows_of(k):
        rows = lax.dynamic_slice_in_dim(padded, ((tp + k) % count) * own, own + halo, 0)
        return jnp.concatenate([rows, *taps], axis=0)

    blocks = (
        rows_of(0),
        over_tp(rows_of(count - 1), -1),
        over_tp(rows_of(1), 1),
        over_tp(rows_of(2), 2),
    )
    activated = call(
        functools.partial(conv_kernel_body, reach, halo),
        shape(own, part * count),
        [VMEM] * 4,
        10**9,
        8,
        [pltpu.VMEM((own + halo, 128), f32), pltpu.VMEM((own, part * count), f32)],
    )(*blocks)
    return call(
        mix_kernel,
        shape(own, 2 * columns),
        [SMEM] + [VMEM] * 6,
        2 * own * part * count * 2 * columns,
        8,
    )(core.astype(jnp.int32).reshape(1), activated, out_weight, *near, far)


def expert_half(moe_input, moe_gain, gate_weight, up_weight, down_weight, expert_ids, route_weight):
    tokens, width = moe_input.shape
    experts = lax.axis_size("ep")
    count = lax.axis_size("tp")
    capacity = 4 * max(1, tokens // experts)
    chunks = 2
    per_chunk = capacity // chunks
    rows = experts * per_chunk
    half = rows // 2
    part = width // count
    tp = lax.axis_index("tp").astype(jnp.int32).reshape(1)
    ids = expert_ids.T

    def exchange(value):
        value = value.reshape(experts, per_chunk, part)
        moved = lax.all_to_all(value, "ep", split_axis=0, concat_axis=0, tiled=True)
        return moved.reshape(rows, part)

    sent = call(
        functools.partial(dispatch_kernel, per_chunk),
        [shape(rows, part)] * chunks,
        [SMEM, ANY, ANY, ANY],
        2 * 2 * rows * tokens * part,
        56,
        [
            pltpu.VMEM((tokens, width), bf16),
            pltpu.VMEM((1, width), f32),
            pltpu.VMEM(ids.shape, jnp.int32),
            pltpu.SemaphoreType.DMA((3,)),
        ],
    )(tp, moe_input, moe_gain.reshape(1, width), ids)
    high, low = call(
        functools.partial(route_kernel, per_chunk),
        [shape(tokens, experts * capacity)] * 2,
        [VMEM, VMEM],
        2 * 2 * rows * tokens * part,
        12,
    )(ids, route_weight.T)
    weights = (gate_weight[0], up_weight[0], down_weight[0])
    whole, halves = shape(rows, part), shape(half, part)

    def run(chunk, outs, blocks):
        return call(
            functools.partial(expert_kernel, chunk),
            outs,
            [SMEM] + [VMEM] * len(blocks) + [ANY] * 3,
            6 * rows * width * gate_weight.shape[2],
            50,
            [pltpu.VMEM(w.shape, bf16) for w in weights]
            + [pltpu.VMEM((rows, part), bf16)] * 3
            + [pltpu.SemaphoreType.DMA((2 * count + 1,))],
        )(tp, *blocks, *weights)

    def fold(kernel, kind, *terms):
        return call(kernel, [kind] * 2, [VMEM] * 4, 10**8, 8)(*terms)

    def total(kernel, *terms):
        return call(kernel, whole, [VMEM] * len(terms), 10**8, 8)(*terms)

    arrived = exchange(sent[0])
    others = gather_direct(arrived)
    own, ahead, behind, top, bottom = run(0, [whole] * 3 + [halves] * 2, (arrived, *others))
    top = over_tp(top, 1)
    bottom = over_tp(bottom, -1)
    ahead, behind = fold(fold_whole_kernel, whole, ahead, top, behind, bottom)
    ahead = over_tp(ahead, 1)
    behind = over_tp(behind, -1)
    answer = total(total_whole_kernel, own, ahead, behind)
    answers = [exchange(answer)]
    arrived = exchange(sent[1])
    others = gather_relayed(arrived)
    own, ahead0, ahead1, behind0, behind1, across0, across1 = run(
        1, [whole] + [halves] * 6, (arrived, *others)
    )
    across0 = over_tp(across0, 1)
    across1 = over_tp(across1, -1)
    bottom0 = over_tp(ahead1, 1)
    top0 = over_tp(behind0, -1)
    ahead0, behind1 = fold(fold_kernel, halves, ahead0, across0, behind1, across1)
    top1 = over_tp(ahead0, 1)
    bottom1 = over_tp(behind1, -1)
    answer = total(total_kernel, own, top0, top1, bottom0, bottom1)
    answers.append(exchange(answer))
    return call(
        combine_kernel,
        shape(tokens, part),
        [VMEM, VMEM, ANY, ANY],
        4 * tokens * rows * part,
        56,
        [pltpu.VMEM((rows, part), bf16)] * 2 + [pltpu.SemaphoreType.DMA((2,))],
    )(high, low, *answers)


def on_device(
    glu_value,
    glu_gate,
    conv_kernel,
    ln_gain,
    out_weight,
    moe_input,
    moe_gain,
    gate_weight,
    up_weight,
    down_weight,
    expert_ids,
    route_weight,
):
    mixer_out = mixer_half(glu_value, glu_gate, conv_kernel, ln_gain, out_weight)
    expert_out = expert_half(
        moe_input, moe_gain, gate_weight, up_weight, down_weight, expert_ids, route_weight
    )
    return (mixer_out, expert_out)


def solution(mesh):
    in_specs = (
        P("ep", "tp"),
        P("ep", "tp"),
        P(None, "tp"),
        P("tp"),
        P("tp", None),
        P("ep", None),
        P(),
        P("ep", None, "tp"),
        P("ep", None, "tp"),
        P("ep", "tp", None),
        P("ep", None),
        P("ep", None),
    )
    out_specs = (P(("ep", "tp"), None), P("ep", "tp"))

    return jax.shard_map(on_device, mesh=mesh, in_specs=in_specs, out_specs=out_specs, check_vma=False)
```

time: 244 us -> 220 us (0.902)
  the two profiles are of different devices: /device:TPU:1 before, /device:TPU:96 now
where the time goes in v1:
time: 220 us; the launch traced here: 219 us
  waiting for transfers between devices  83.5 us (38%)
  starting transfers between devices  59.6 us (27%)
  Pallas kernels  33.4 us (15%)
  blocking collectives  28 us (13%)
  local copies, waits for them, and re-layouts  11 us (5%)
  other arithmetic  2.6 us (1%)
    ppermute x23, waiting for transfers between devices, over_tp(): lax.ppermute(value, 'tp', [(i, (i + by) % count) for i in range(count)])  72 us
    ppermute x23, starting transfers between devices, over_tp(): lax.ppermute(value, 'tp', [(i, (i + by) % count) for i in range(count)])  30.5 us
    all_to_all x1, blocking collectives, exchange(): moved = lax.all_to_all(value, 'ep', split_axis=0, concat_axis=0, tiled=True)  28 us
    all_to_all x3, starting transfers between devices, exchange(): moved = lax.all_to_all(value, 'ep', split_axis=0, concat_axis=0, tiled=True)  27.1 us
    pallas_call x2, Pallas kernels, run(): call(functools.partial(expert_kernel, chunk), outs, [SMEM] + [VMEM] * len...  18.4 us
    ppermute x1, waiting for transfers between devices, from_behind(): return lax.ppermute(value, axis, [(i, i + by) for i in range(count - by)])  11.5 us
    unnamed x40, local copies, waits for them, and re-layouts  10.1 us
  transfers between devices with their start and end apart: 28, of which 14 were waited for; matrix products, arithmetic and copies ran while one was open for 2% of the time, Pallas kernels for 12%

profile of v1, /device:TPU:96, one launch (start us, length us, event | category | flops | bytes accessed | tf_op | source)
XLA Modules:
  0.0 219.2 jit_solution(17772116626309517927)
XLA Ops:
  0.6 2.9 %shard_map.134 = (bf16[512,512]{1,0:T(8,128)(2,1)}, bf16[512,512]{1,0:T(8,128)(2,1)}) custom-call(s32[1]{0:T(128)} %bitcast.4.tp_ref, bf16[256,2048]{1,0:T(8,128)(2,1)} %x_hbm.1, f32[1,2048]{1,0:T(1,128)} %bitcast.30, s32[2,256]{1,0:T(2,128)} %bitcast.24), custom_call_target="tpu_custom_call" | custom-call | flops 268435456 | bytes 1048576 | tf_op jit(solution)/shard_map/pallas_call | solution.py:351
  3.6 28.0 %all_to_all.20 = bf16[64,8,512]{2,1,0:T(8,128)(2,1)S(1)} all-to-all(bf16[64,8,512]{2,1,0:T(8,128)(2,1)} %bitcast.29), channel_id=1, replica_groups=mesh['ep'=64,'tp'=4] {'ep'}, dimensions={0} | all-to-all | bytes 1048576 | tf_op jit(solution)/shard_map/all_to_all | solution.py:348
  31.5 6.3 %all-to-all-start = ((bf16[64,8,512]{2,1,0:T(8,128)(2,1)}), bf16[64,8,512]{2,1,0:T(8,128)(2,1)S(1)}, u32[]{:S(2)}, u32[]{:S(2)}) async-start(bf16[64,8,512]{2,1,0:T(8,128)(2,1)} %bitcast.28), calls=%async_computation | async-start | bytes 1048576 | tf_op jit(solution)/shard_map/all_to_all | solution.py:348
  37.8 2.8 %collective-permute-start.15 = (bf16[512,512]{1,0:T(8,128)(2,1)S(1)}, bf16[512,512]{1,0:T(8,128)(2,1)S(1)}, u32[]{:S(2)}, u32[]{:S(2)}) collective-permute-start(bf16[512,512]{1,0:T(8,128)(2,1)S(1)} %bitcast.21), channel_id=1, source_target_pairs={{0,3},{1,0},{2,1},{3,2},{4,7},{5,4},{6,5},{7,6},{8,11},{9,8},{10,9... | collective-permute-start | bytes 1572872 | tf_op jit(solution)/shard_map/ppermute | solution.py:28
  40.7 11.5 %collective-permute-done.15.ahead = bf16[512,512]{1,0:T(8,128)(2,1)S(1)} collective-permute-done((bf16[512,512]{1,0:T(8,128)(2,1)S(1)}, bf16[512,512]{1,0:T(8,128)(2,1)S(1)}, u32[]{:S(2)}, u32[]{:S(2)}) %collective-permute-start.15) | collective-permute-done | bytes 524320 | tf_op jit(solution)/shard_map/ppermute | solution.py:28
  52.2 3.8 %collective-permute-start.17 = (bf16[256,512]{1,0:T(8,128)(2,1)S(1)}, bf16[256,512]{1,0:T(8,128)(2,1)S(1)}, u32[]{:S(2)}, u32[]{:S(2)}) collective-permute-start(bf16[256,512]{1,0:T(8,128)(2,1)S(1)} %slice.13), channel_id=1, source_target_pairs={{0,3},{1,0},{2,1},{3,2},{4,7},{5,4},{6,5},{7,6},{8,11},{9,8},{10,9... | collective-permute-start | bytes 786440 | tf_op jit(solution)/shard_map/ppermute | solution.py:28
  56.1 1.9 collective-permute-start.10
  58.0 14.2 %collective-permute-done.17.refs_0_ = bf16[256,512]{1,0:T(8,128)(2,1)S(1)} collective-permute-done((bf16[256,512]{1,0:T(8,128)(2,1)S(1)}, bf16[256,512]{1,0:T(8,128)(2,1)S(1)}, u32[]{:S(2)}, u32[]{:S(2)}) %collective-permute-start.17) | collective-permute-done | bytes 262176 | tf_op jit(solution)/shard_map/ppermute | solution.py:28
  72.2 3.5 %collective-permute-done.18.refs_1_ = bf16[256,512]{1,0:T(8,128)(2,1)S(1)} collective-permute-done((bf16[256,512]{1,0:T(8,128)(2,1)S(1)}, bf16[256,512]{1,0:T(8,128)(2,1)S(1)}, u32[]{:S(2)}, u32[]{:S(2)}) %collective-permute-start.18) | collective-permute-done | bytes 262176 | tf_op jit(solution)/shard_map/ppermute | solution.py:28
  76.4 0.9 copy-done.13
  77.4 9.1 %shard_map.138 = (bf16[512,512]{1,0:T(8,128)(2,1)S(1)}, bf16[256,512]{1,0:T(8,128)(2,1)S(1)}, bf16[256,512]{1,0:T(8,128)(2,1)S(1)}, bf16[256,512]{1,0:T(8,128)(2...) custom-call(s32[1]{0:T(128)} %bitcast.4.tp_ref, ...), custom_call_target="tpu_custom_call" | custom-call | flops 4831838208 | bytes 1048576 | tf_op jit(solution)/shard_map/pallas_call | solution.py:375
  86.6 3.2 %collective-permute-start.21 = (bf16[256,512]{1,0:T(8,128)(2,1)S(1)}, bf16[256,512]{1,0:T(8,128)(2,1)S(1)}, u32[]{:S(2)}, u32[]{:S(2)}) collective-permute-start(bf16[256,512]{1,0:T(8,128)(2,1)S(1)} %get-tuple-element.38), channel_id=1, source_target_pairs={{0,3},{1,0},{2,1},{3,2},{4,7},{5,4},{6,5},{7,6},{8,11},{9,8},{10,9... | collective-permute-start | bytes 786440 | tf_op jit(solution)/shard_map/ppermute | solution.py:28
  89.8 6.0 %collective-permute-done.20.b = bf16[256,512]{1,0:T(8,128)(2,1)S(1)} collective-permute-done((bf16[256,512]{1,0:T(8,128)(2,1)S(1)}, bf16[256,512]{1,0:T(8,128)(2,1)S(1)}, u32[]{:S(2)}, u32[]{:S(2)}) %collective-permute-start.20) | collective-permute-done | bytes 262176 | tf_op jit(solution)/shard_map/ppermute | solution.py:28
  97.3 1.9 collective-permute-start.22
  99.2 2.9 %collective-permute-done.19.top0 = bf16[256,512]{1,0:T(8,128)(2,1)S(1)} collective-permute-done((bf16[256,512]{1,0:T(8,128)(2,1)S(1)}, bf16[256,512]{1,0:T(8,128)(2,1)S(1)}, u32[]{:S(2)}, u32[]{:S(2)}) %collective-permute-start.19) | collective-permute-done | bytes 262176 | tf_op jit(solution)/shard_map/ppermute | solution.py:28
  102.1 3.7 %collective-permute-start.24 = (bf16[256,512]{1,0:T(8,128)(2,1)}, bf16[256,512]{1,0:T(8,128)(2,1)S(1)}, u32[]{:S(2)}, u32[]{:S(2)}) collective-permute-start(bf16[256,512]{1,0:T(8,128)(2,1)} %get-tuple-element.41), channel_id=1, source_target_pairs={{0,3},{1,0},{2,1},{3,2},{4,7},{5,4},{6,5},{7,6},{8,11},{9,8},{10,9... | collective-permute-start | bytes 786440 | tf_op jit(solution)/shard_map/ppermute | solution.py:28
  105.8 0.8 constant_dynamic-slice_fusion
  106.6 7.2 %collective-permute-done.23.bottom0 = bf16[256,512]{1,0:T(8,128)(2,1)S(1)} collective-permute-done((bf16[256,512]{1,0:T(8,128)(2,1)S(1)}, bf16[256,512]{1,0:T(8,128)(2,1)S(1)}, u32[]{:S(2)}, u32[]{:S(2)}) %collective-permute-start.23) | collective-permute-done | bytes 262176 | tf_op jit(solution)/shard_map/ppermute | solution.py:28
  114.5 3.6 %collective-permute-done.22.top1 = bf16[256,512]{1,0:T(8,128)(2,1)S(1)} collective-permute-done((bf16[256,512]{1,0:T(8,128)(2,1)S(1)}, bf16[256,512]{1,0:T(8,128)(2,1)S(1)}, u32[]{:S(2)}, u32[]{:S(2)}) %collective-permute-start.22) | collective-permute-done | bytes 262176 | tf_op jit(solution)/shard_map/ppermute | solution.py:28
  118.9 1.1 collective-permute-done.24.bottom1
  120.7 0.9 collective-permute-start.6
  121.6 1.0 copy-done.2
  122.6 0.9 copy-done.6
  123.6 0.9 copy-done.8
  124.5 0.9 copy-done.10
  125.5 1.0 shard_map.140
  126.5 10.5 %all-to-all-start.3 = ((bf16[64,8,512]{2,1,0:T(8,128)(2,1)}), bf16[64,8,512]{2,1,0:T(8,128)(2,1)}, u32[]{:S(2)}, u32[]{:S(2)}) async-start(bf16[64,8,512]{2,1,0:T(8,128)(2,1)} %bitcast.15), calls=%async_computation.3 | async-start | bytes 1048576 | tf_op jit(solution)/shard_map/all_to_all | solution.py:348
  137.0 9.3 %shard_map.135 = (bf16[512,512]{1,0:T(8,128)(2,1)S(1)}, bf16[512,512]{1,0:T(8,128)(2,1)S(1)}, bf16[512,512]{1,0:T(8,128)(2,1)S(1)}, bf16[256,512]{1,0:T(8,128)(2,1)S(1)}, bf16[256,512]{1,0:T(8,128)(2,1)S(1)}) custom-call(s32[1]{0:T(128)} %bitcast.4.tp_ref, bf16[512,512]{1,0:T(8,128)(2,1)S(1)} %bitcast.20, bf16[512,512]{1,0:T(8,128)(2,1)} %collective-permute-done.8.ahead, ...), custom_call_target="tpu_custom_call" | custom-call | flops 4831838208 | bytes 1048576 | tf_op jit(solution)/shard_map/pallas_call | solution.py:375
  146.3 4.1 %collective-permute-start.11 = (bf16[256,512]{1,0:T(8,128)(2,1)S(1)}, bf16[256,512]{1,0:T(8,128)(2,1)S(1)}, u32[]{:S(2)}, u32[]{:S(2)}) collective-permute-start(bf16[256,512]{1,0:T(8,128)(2,1)S(1)} %get-tuple-element.27), channel_id=1, source_target_pairs={{0,1},{1,2},{2,3},{3,0},{4,5},{5,6},{6,7},{7,4},{8,9},{9,10},{10,1... | collective-permute-start | bytes 786440 | tf_op jit(solution)/shard_map/ppermute | solution.py:28
  150.4 1.3 pad_maximum_fusion
  151.6 4.6 %collective-permute-done.11.top = bf16[256,512]{1,0:T(8,128)(2,1)S(1)} collective-permute-done((bf16[256,512]{1,0:T(8,128)(2,1)S(1)}, bf16[256,512]{1,0:T(8,128)(2,1)S(1)}, u32[]{:S(2)}, u32[]{:S(2)}) %collective-permute-start.11) | collective-permute-done | bytes 262176 | tf_op jit(solution)/shard_map/ppermute | solution.py:28
  156.2 2.2 %collective-permute-done.12.bottom = bf16[256,512]{1,0:T(8,128)(2,1)S(1)} collective-permute-done((bf16[256,512]{1,0:T(8,128)(2,1)S(1)}, bf16[256,512]{1,0:T(8,128)(2,1)S(1)}, u32[]{:S(2)}, u32[]{:S(2)}) %collective-permute-start.12) | collective-permute-done | bytes 262176 | tf_op jit(solution)/shard_map/ppermute | solution.py:28
  159.0 2.9 %collective-permute-start.14 = (bf16[512,512]{1,0:T(8,128)(2,1)S(1)}, bf16[512,512]{1,0:T(8,128)(2,1)S(1)}, u32[]{:S(2)}, u32[]{:S(2)}) collective-permute-start(bf16[512,512]{1,0:T(8,128)(2,1)S(1)} %get-tuple-element.31), channel_id=1, source_target_pairs={{0,3},{1,0},{2,1},{3,2},{4,7},{5,4},{6,5},{7,6},{8,11},{9,8},{10,9... | collective-permute-start | bytes 1572872 | tf_op jit(solution)/shard_map/ppermute | solution.py:28
  161.9 10.8 %collective-permute-done.13.first = bf16[512,512]{1,0:T(8,128)(2,1)S(1)} collective-permute-done((bf16[512,512]{1,0:T(8,128)(2,1)S(1)}, bf16[512,512]{1,0:T(8,128)(2,1)S(1)}, u32[]{:S(2)}, u32[]{:S(2)}) %collective-permute-start.13) | collective-permute-done | bytes 524320 | tf_op jit(solution)/shard_map/ppermute | solution.py:28
  172.7 1.0 shard_map.137
  173.7 10.3 %all-to-all-start.1 = ((bf16[64,8,512]{2,1,0:T(8,128)(2,1)}), bf16[64,8,512]{2,1,0:T(8,128)(2,1)S(1)}, u32[]{:S(2)}, u32[]{:S(2)}) async-start(bf16[64,8,512]{2,1,0:T(8,128)(2,1)} %bitcast.11), calls=%async_computation.1 | async-start | bytes 1048576 | tf_op jit(solution)/shard_map/all_to_all | solution.py:348
  184.0 1.2 multiply_convert_fusion
  185.2 2.0 collective-permute-start
  187.3 11.5 %collective-permute-done = bf16[32,256]{1,0:T(8,128)(2,1)S(1)} collective-permute-done((bf16[32,256]{1,0:T(8,128)(2,1)S(1)}, bf16[32,256]{1,0:T(8,128)(2,1)S(1)}, u32[]{:S(2)}, u32[]{:S(2)}) %collective-permute-start) | collective-permute-done | bytes 16416 | tf_op jit(solution)/shard_map/ppermute | solution.py:33
  199.0 3.0 %collective-permute-start.1 = (bf16[256,256]{1,0:T(8,128)(2,1)S(1)}, bf16[256,256]{1,0:T(8,128)(2,1)S(1)}, u32[]{:S(2)}, u32[]{:S(2)}) collective-permute-start(bf16[256,256]{1,0:T(8,128)(2,1)S(1)} %get-tuple-element.47), channel_id=1, source_target_pairs={{0,3},{1,0},{2,1},{3,2},{4,7},{5,4},{6,5},{7,6},{8,11},{9,8},{10,9... | collective-permute-start | bytes 393224 | tf_op jit(solution)/shard_map/ppermute | solution.py:28
  202.0 1.6 collective-permute-start.3
  204.1 0.8 copy-done.3
  204.9 0.8 copy-done.4
  205.7 3.8 %collective-permute-done.2.b2 = bf16[256,256]{1,0:T(8,128)(2,1)S(1)} collective-permute-done((bf16[256,256]{1,0:T(8,128)(2,1)S(1)}, bf16[256,256]{1,0:T(8,128)(2,1)S(1)}, u32[]{:S(2)}, u32[]{:S(2)}) %collective-permute-start.2) | collective-permute-done | bytes 131104 | tf_op jit(solution)/shard_map/ppermute | solution.py:28
  209.6 2.0 shard_map.131.act
  211.6 2.9 %shard_map.132 = bf16[128,2048]{1,0:T(8,128)(2,1)} custom-call(s32[1]{0:T(128)} %bitcast.core_ref, bf16[128,1024]{1,0:T(8,128)(2,1)S(1)} %shard_map.131.act, bf16[256,2048]{1,0:T(8,128)(2,1)S(1)} %copy-done, bf16[256,1024]{1,0:T(8,128)(2,1)S(1)} %collective-permute-done.4.n1, bf16[256,1024]{1,0:T(8,128)(2,1)S(1)} %collective-permute-done.5.n2, ...), custom_call_target="tpu_custom_call" | custom-call | flops 536870912 | bytes 1048576 | tf_op jit(solution)/shard_map/pallas_call | solution.py:324
  214.5 0.8 copy-done.15
  215.3 3.7 %shard_map.141 = bf16[256,512]{1,0:T(8,128)(2,1)} custom-call(bf16[256,1024]{1,0:T(8,128)(2,1)} %copy-done.3, bf16[256,1024]{1,0:T(8,128)(2,1)} %copy-done.4, bf16[512,512]{1,0:T(8,128)(2,1)} %bitcast.27, bf16[512,512]{1,0:T(8,128)(2,1)} %bitcast.16.a1_hbm), custom_call_target="tpu_custom_call" | custom-call | flops 268435456 | bytes 1048576 | tf_op jit(solution)/shard_map/pallas_call | solution.py:416
  (70 shorter events, 5.9 us)
Async XLA Ops:
  31.5 24.5 %all-to-all-start = ((bf16[64,8,512]{2,1,0:T(8,128)(2,1)}), bf16[64,8,512]{2,1,0:T(8,128)(2,1)S(1)}, u32[]{:S(2)}, u32[]{:S(2)}) async-start(bf16[64,8,512]{2,1,0:T(8,128)(2,1)} %bitcast.28), calls=%async_computation | async-start | bytes 1048576 | tf_op jit(solution)/shard_map/all_to_all | solution.py:348
  37.8 14.3 %collective-permute-start.15 = (bf16[512,512]{1,0:T(8,128)(2,1)S(1)}, bf16[512,512]{1,0:T(8,128)(2,1)S(1)}, u32[]{:S(2)}, u32[]{:S(2)}) collective-permute-start(bf16[512,512]{1,0:T(8,128)(2,1)S(1)} %bitcast.21), channel_id=1, source_target_pairs={{0,3},{1,0},{2,1},{3,2},{4,7},{5,4},{6,5},{7,6},{8,11},{9,8},{10,9... | collective-permute-start | bytes 1572872 | tf_op jit(solution)/shard_map/ppermute | solution.py:28
  40.7 15.3 %collective-permute-start.16 = (bf16[512,512]{1,0:T(8,128)(2,1)S(1)}, bf16[512,512]{1,0:T(8,128)(2,1)S(1)}, u32[]{:S(2)}, u32[]{:S(2)}) collective-permute-start(bf16[512,512]{1,0:T(8,128)(2,1)S(1)} %bitcast.22), channel_id=1, source_target_pairs={{0,1},{1,2},{2,3},{3,0},{4,5},{5,6},{6,7},{7,4},{8,9},{9,10},{10,1... | collective-permute-start | bytes 1572872 | tf_op jit(solution)/shard_map/ppermute | solution.py:28
  52.2 20.0 %collective-permute-start.17 = (bf16[256,512]{1,0:T(8,128)(2,1)S(1)}, bf16[256,512]{1,0:T(8,128)(2,1)S(1)}, u32[]{:S(2)}, u32[]{:S(2)}) collective-permute-start(bf16[256,512]{1,0:T(8,128)(2,1)S(1)} %slice.13), channel_id=1, source_target_pairs={{0,3},{1,0},{2,1},{3,2},{4,7},{5,4},{6,5},{7,6},{8,11},{9,8},{10,9... | collective-permute-start | bytes 786440 | tf_op jit(solution)/shard_map/ppermute | solution.py:28
  55.9 20.4 %copy-start.16 = (bf16[512,512]{1,0:T(8,128)(2,1)}, bf16[512,512]{1,0:T(8,128)(2,1)S(1)}, u32[]{:S(2)}) copy-start(bf16[512,512]{1,0:T(8,128)(2,1)S(1)} %collective-permute-done.16.behind) | copy-start | bytes 1572868
  56.0 19.7 %collective-permute-start.18 = (bf16[256,512]{1,0:T(8,128)(2,1)S(1)}, bf16[256,512]{1,0:T(8,128)(2,1)S(1)}, u32[]{:S(2)}, u32[]{:S(2)}) collective-permute-start(bf16[256,512]{1,0:T(8,128)(2,1)S(1)} %slice.14), channel_id=1, source_target_pairs={{0,1},{1,2},{2,3},{3,0},{4,5},{5,6},{6,7},{7,4},{8,9},{9,10},{10,1... | collective-permute-start | bytes 786440 | tf_op jit(solution)/shard_map/ppermute | solution.py:28
  56.1 41.2 %collective-permute-start.10 = (bf16[512,512]{1,0:T(8,128)(2,1)S(1)}, bf16[512,512]{1,0:T(8,128)(2,1)S(1)}, u32[]{:S(2)}, u32[]{:S(2)}) collective-permute-start(bf16[512,512]{1,0:T(8,128)(2,1)S(1)} %bitcast.17), channel_id=1, source_target_pairs={{0,2},{1,3},{2,0},{3,1},{4,6},{5,7},{6,4},{7,5},{8,10},{9,11},{10,... | collective-permute-start | bytes 1572872 | tf_op jit(solution)/shard_map/ppermute | solution.py:28
  75.7 0.7 copy-start.12
  76.4 1.0 copy-start.13
  77.3 28.5 %copy-start = (bf16[256,2048]{1,0:T(8,128)(2,1)S(1)}, bf16[256,2048]{1,0:T(8,128)(2,1)}, u32[]{:S(2)}) copy-start(bf16[256,2048]{1,0:T(8,128)(2,1)} %own.1) | copy-start | bytes 3145732
  86.5 10.8 %copy-start.1 = (bf16[512,512]{1,0:T(8,128)(2,1)}, bf16[512,512]{1,0:T(8,128)(2,1)S(1)}, u32[]{:S(2)}) copy-start(bf16[512,512]{1,0:T(8,128)(2,1)S(1)} %get-tuple-element.33.own) | copy-start | bytes 1572868
  86.5 9.4 %collective-permute-start.20 = (bf16[256,512]{1,0:T(8,128)(2,1)S(1)}, bf16[256,512]{1,0:T(8,128)(2,1)S(1)}, u32[]{:S(2)}, u32[]{:S(2)}) collective-permute-start(bf16[256,512]{1,0:T(8,128)(2,1)S(1)} %get-tuple-element.36), channel_id=1, source_target_pairs={{0,1},{1,2},{2,3},{3,0},{4,5},{5,6},{6,7},{7,4},{8,9},{9,10},{10,1... | collective-permute-start | bytes 786440 | tf_op jit(solution)/shard_map/ppermute | solution.py:28
  86.6 9.9 %collective-permute-start.21 = (bf16[256,512]{1,0:T(8,128)(2,1)S(1)}, bf16[256,512]{1,0:T(8,128)(2,1)S(1)}, u32[]{:S(2)}, u32[]{:S(2)}) collective-permute-start(bf16[256,512]{1,0:T(8,128)(2,1)S(1)} %get-tuple-element.38), channel_id=1, source_target_pairs={{0,3},{1,0},{2,1},{3,2},{4,7},{5,4},{6,5},{7,6},{8,11},{9,8},{10,9... | collective-permute-start | bytes 786440 | tf_op jit(solution)/shard_map/ppermute | solution.py:28
  89.8 12.3 %collective-permute-start.19 = (bf16[256,512]{1,0:T(8,128)(2,1)S(1)}, bf16[256,512]{1,0:T(8,128)(2,1)S(1)}, u32[]{:S(2)}, u32[]{:S(2)}) collective-permute-start(bf16[256,512]{1,0:T(8,128)(2,1)S(1)} %get-tuple-element.34), channel_id=1, source_target_pairs={{0,3},{1,0},{2,1},{3,2},{4,7},{5,4},{6,5},{7,6},{8,11},{9,8},{10,9... | collective-permute-start | bytes 786440 | tf_op jit(solution)/shard_map/ppermute | solution.py:28
  89.8 47.1 %collective-permute-start.8 = (bf16[512,512]{1,0:T(8,128)(2,1)S(1)}, bf16[512,512]{1,0:T(8,128)(2,1)}, u32[]{:S(2)}, u32[]{:S(2)}) collective-permute-start(bf16[512,512]{1,0:T(8,128)(2,1)S(1)} %bitcast.18), channel_id=1, source_target_pairs={{0,3},{1,0},{2,1},{3,2},{4,7},{5,4},{6,5},{7,6},{8,11},{9,8},{10,9... | collective-permute-start | bytes 1572872 | tf_op jit(solution)/shard_map/ppermute | solution.py:28
  95.9 41.1 %collective-permute-start.9 = (bf16[512,512]{1,0:T(8,128)(2,1)S(1)}, bf16[512,512]{1,0:T(8,128)(2,1)}, u32[]{:S(2)}, u32[]{:S(2)}) collective-permute-start(bf16[512,512]{1,0:T(8,128)(2,1)S(1)} %bitcast.19), channel_id=1, source_target_pairs={{0,1},{1,2},{2,3},{3,0},{4,5},{5,6},{6,7},{7,4},{8,9},{9,10},{10,1... | collective-permute-start | bytes 1572872 | tf_op jit(solution)/shard_map/ppermute | solution.py:28
  96.5 17.3 %collective-permute-start.23 = (bf16[256,512]{1,0:T(8,128)(2,1)S(1)}, bf16[256,512]{1,0:T(8,128)(2,1)S(1)}, u32[]{:S(2)}, u32[]{:S(2)}) collective-permute-start(bf16[256,512]{1,0:T(8,128)(2,1)S(1)} %get-tuple-element.40), channel_id=1, source_target_pairs={{0,1},{1,2},{2,3},{3,0},{4,5},{5,6},{6,7},{7,4},{8,9},{9,10},{10,1... | collective-permute-start | bytes 786440 | tf_op jit(solution)/shard_map/ppermute | solution.py:28
  97.3 4.8 %copy-start.19 = (bf16[512,512]{1,0:T(8,128)(2,1)}, bf16[512,512]{1,0:T(8,128)(2,1)S(1)}, u32[]{:S(2)}) copy-start(bf16[512,512]{1,0:T(8,128)(2,1)S(1)} %collective-permute-done.10.refs_0_) | copy-start | bytes 1572868
  97.3 20.9 %collective-permute-start.22 = (bf16[256,512]{1,0:T(8,128)(2,1)S(1)}, bf16[256,512]{1,0:T(8,128)(2,1)S(1)}, u32[]{:S(2)}, u32[]{:S(2)}) collective-permute-start(bf16[256,512]{1,0:T(8,128)(2,1)S(1)} %get-tuple-element.39), channel_id=1, source_target_pairs={{0,1},{1,2},{2,3},{3,0},{4,5},{5,6},{6,7},{7,4},{8,9},{9,10},{10,1... | collective-permute-start | bytes 786440 | tf_op jit(solution)/shard_map/ppermute | solution.py:28
  102.1 17.8 %collective-permute-start.24 = (bf16[256,512]{1,0:T(8,128)(2,1)}, bf16[256,512]{1,0:T(8,128)(2,1)S(1)}, u32[]{:S(2)}, u32[]{:S(2)}) collective-permute-start(bf16[256,512]{1,0:T(8,128)(2,1)} %get-tuple-element.41), channel_id=1, source_target_pairs={{0,3},{1,0},{2,1},{3,2},{4,7},{5,4},{6,5},{7,6},{8,11},{9,8},{10,9... | collective-permute-start | bytes 786440 | tf_op jit(solution)/shard_map/ppermute | solution.py:28
  113.8 0.7 copy-start.5
  114.5 35.8 %collective-permute-start.4 = (bf16[256,1024]{1,0:T(8,128)(2,1)}, bf16[256,1024]{1,0:T(8,128)(2,1)S(1)}, u32[]{:S(2)}, u32[]{:S(2)}) collective-permute-start(bf16[256,1024]{1,0:T(8,128)(2,1)} %constant_dynamic-slice_fusion), channel_id=1, source_target_pairs={{0,3},{1,0},{2,1},{3,2},{4,7},{5,4},{6,5},{7,6},{8,11},{9,8},{10,9... | collective-permute-start | bytes 1572872 | tf_op jit(solution)/shard_map/ppermute | solution.py:28
  118.1 0.7 copy-start.7
  118.9 31.5 %collective-permute-start.5 = (bf16[256,1024]{1,0:T(8,128)(2,1)}, bf16[256,1024]{1,0:T(8,128)(2,1)S(1)}, u32[]{:S(2)}, u32[]{:S(2)}) collective-permute-start(bf16[256,1024]{1,0:T(8,128)(2,1)} %constant_dynamic-slice_fusion), channel_id=1, source_target_pairs={{0,1},{1,2},{2,3},{3,0},{4,5},{5,6},{6,7},{7,4},{8,9},{9,10},{10,1... | collective-permute-start | bytes 1572872 | tf_op jit(solution)/shard_map/ppermute | solution.py:28
  120.0 0.7 copy-start.9
  120.7 29.7 %collective-permute-start.6 = (bf16[256,1024]{1,0:T(8,128)(2,1)}, bf16[256,1024]{1,0:T(8,128)(2,1)S(1)}, u32[]{:S(2)}, u32[]{:S(2)}) collective-permute-start(bf16[256,1024]{1,0:T(8,128)(2,1)} %constant_dynamic-slice_fusion), channel_id=1, source_target_pairs={{0,2},{1,3},{2,0},{3,1},{4,6},{5,7},{6,4},{7,5},{8,10},{9,11},{10,... | collective-permute-start | bytes 1572872 | tf_op jit(solution)/shard_map/ppermute | solution.py:28
  121.6 1.0 copy-start.2
  122.6 0.9 copy-start.6
  123.6 0.9 copy-start.8
  124.5 0.9 copy-start.10
  126.5 47.2 %all-to-all-start.3 = ((bf16[64,8,512]{2,1,0:T(8,128)(2,1)}), bf16[64,8,512]{2,1,0:T(8,128)(2,1)}, u32[]{:S(2)}, u32[]{:S(2)}) async-start(bf16[64,8,512]{2,1,0:T(8,128)(2,1)} %bitcast.15), calls=%async_computation.3 | async-start | bytes 1048576 | tf_op jit(solution)/shard_map/all_to_all | solution.py:348
  146.3 9.9 %collective-permute-start.11 = (bf16[256,512]{1,0:T(8,128)(2,1)S(1)}, bf16[256,512]{1,0:T(8,128)(2,1)S(1)}, u32[]{:S(2)}, u32[]{:S(2)}) collective-permute-start(bf16[256,512]{1,0:T(8,128)(2,1)S(1)} %get-tuple-element.27), channel_id=1, source_target_pairs={{0,1},{1,2},{2,3},{3,0},{4,5},{5,6},{6,7},{7,4},{8,9},{9,10},{10,1... | collective-permute-start | bytes 786440 | tf_op jit(solution)/shard_map/ppermute | solution.py:28
  150.3 8.1 %collective-permute-start.12 = (bf16[256,512]{1,0:T(8,128)(2,1)S(1)}, bf16[256,512]{1,0:T(8,128)(2,1)S(1)}, u32[]{:S(2)}, u32[]{:S(2)}) collective-permute-start(bf16[256,512]{1,0:T(8,128)(2,1)S(1)} %get-tuple-element.29), channel_id=1, source_target_pairs={{0,3},{1,0},{2,1},{3,2},{4,7},{5,4},{6,5},{7,6},{8,11},{9,8},{10,9... | collective-permute-start | bytes 786440 | tf_op jit(solution)/shard_map/ppermute | solution.py:28
  151.6 35.6 %copy-start.17 = (f32[31,256]{1,0:T(8,128)S(1)}, f32[31,256]{1,0:T(8,128)}, u32[]{:S(2)}) copy-start(f32[31,256]{1,0:T(8,128)} %param.14) | copy-start | bytes 95236
  151.6 35.6 %copy-start.18 = (f32[256]{0:T(256)S(1)}, f32[256]{0:T(256)}, u32[]{:S(2)}) copy-start(f32[256]{0:T(256)} %param.15) | copy-start | bytes 3076
  151.6 60.0 %collective-permute-start.7 = (bf16[768,1024]{1,0:T(8,128)(2,1)}, bf16[768,1024]{1,0:T(8,128)(2,1)}, u32[]{:S(2)}, u32[]{:S(2)}) collective-permute-start(bf16[768,1024]{1,0:T(8,128)(2,1)} %pad_maximum_fusion), channel_id=1, source_target_pairs={{0,4},{4,0},{8,12},{12,8},{16,20},{20,16},{24,28},{28,24},{32,36},... | collective-permute-start | bytes 4718600 | tf_op jit(solution)/shard_map/ppermute | solution.py:38
  158.5 45.0 %copy-start.11 = (s32[256,2]{0,1:T(2,128)S(1)}, s32[256,2]{0,1:T(2,128)}, u32[]{:S(2)}) copy-start(s32[256,2]{0,1:T(2,128)} %param.22) | copy-start | bytes 6148
  158.5 45.0 %copy-start.14 = (f32[256,2]{0,1:T(2,128)S(1)}, f32[256,2]{0,1:T(2,128)}, u32[]{:S(2)}) copy-start(f32[256,2]{0,1:T(2,128)} %param.23) | copy-start | bytes 6148
  158.6 14.1 %collective-permute-start.13 = (bf16[512,512]{1,0:T(8,128)(2,1)S(1)}, bf16[512,512]{1,0:T(8,128)(2,1)S(1)}, u32[]{:S(2)}, u32[]{:S(2)}) collective-permute-start(bf16[512,512]{1,0:T(8,128)(2,1)S(1)} %get-tuple-element.30), channel_id=1, source_target_pairs={{0,1},{1,2},{2,3},{3,0},{4,5},{5,6},{6,7},{7,4},{8,9},{9,10},{10,1... | collective-permute-start | bytes 1572872 | tf_op jit(solution)/shard_map/ppermute | solution.py:28
  159.0 13.7 %collective-permute-start.14 = (bf16[512,512]{1,0:T(8,128)(2,1)S(1)}, bf16[512,512]{1,0:T(8,128)(2,1)S(1)}, u32[]{:S(2)}, u32[]{:S(2)}) collective-permute-start(bf16[512,512]{1,0:T(8,128)(2,1)S(1)} %get-tuple-element.31), channel_id=1, source_target_pairs={{0,3},{1,0},{2,1},{3,2},{4,7},{5,4},{6,5},{7,6},{8,11},{9,8},{10,9... | collective-permute-start | bytes 1572872 | tf_op jit(solution)/shard_map/ppermute | solution.py:28
  173.7 40.9 %all-to-all-start.1 = ((bf16[64,8,512]{2,1,0:T(8,128)(2,1)}), bf16[64,8,512]{2,1,0:T(8,128)(2,1)S(1)}, u32[]{:S(2)}, u32[]{:S(2)}) async-start(bf16[64,8,512]{2,1,0:T(8,128)(2,1)} %bitcast.11), calls=%async_computation.1 | async-start | bytes 1048576 | tf_op jit(solution)/shard_map/all_to_all | solution.py:348
  185.2 13.6 %collective-permute-start = (bf16[32,256]{1,0:T(8,128)(2,1)S(1)}, bf16[32,256]{1,0:T(8,128)(2,1)S(1)}, u32[]{:S(2)}, u32[]{:S(2)}) collective-permute-start(bf16[32,256]{1,0:T(8,128)(2,1)S(1)} %slice.12), channel_id=1, source_target_pairs={{0,4},{4,8},{8,12},{12,16},{16,20},{20,24},{24,28},{28,32},{32,36}... | collective-permute-start | bytes 49160 | tf_op jit(solution)/shard_map/ppermute | solution.py:33
  199.0 6.8 %collective-permute-start.1 = (bf16[256,256]{1,0:T(8,128)(2,1)S(1)}, bf16[256,256]{1,0:T(8,128)(2,1)S(1)}, u32[]{:S(2)}, u32[]{:S(2)}) collective-permute-start(bf16[256,256]{1,0:T(8,128)(2,1)S(1)} %get-tuple-element.47), channel_id=1, source_target_pairs={{0,3},{1,0},{2,1},{3,2},{4,7},{5,4},{6,5},{7,6},{8,11},{9,8},{10,9... | collective-permute-start | bytes 393224 | tf_op jit(solution)/shard_map/ppermute | solution.py:28
  202.0 7.6 %collective-permute-start.2 = (bf16[256,256]{1,0:T(8,128)(2,1)S(1)}, bf16[256,256]{1,0:T(8,128)(2,1)S(1)}, u32[]{:S(2)}, u32[]{:S(2)}) collective-permute-start(bf16[256,256]{1,0:T(8,128)(2,1)S(1)} %get-tuple-element.48), channel_id=1, source_target_pairs={{0,1},{1,2},{2,3},{3,0},{4,5},{5,6},{6,7},{7,4},{8,9},{9,10},{10,1... | collective-permute-start | bytes 393224 | tf_op jit(solution)/shard_map/ppermute | solution.py:28
  202.0 7.6 %collective-permute-start.3 = (bf16[256,256]{1,0:T(8,128)(2,1)S(1)}, bf16[256,256]{1,0:T(8,128)(2,1)S(1)}, u32[]{:S(2)}, u32[]{:S(2)}) collective-permute-start(bf16[256,256]{1,0:T(8,128)(2,1)S(1)} %get-tuple-element.46), channel_id=1, source_target_pairs={{0,2},{1,3},{2,0},{3,1},{4,6},{5,7},{6,4},{7,5},{8,10},{9,11},{10,... | collective-permute-start | bytes 393224 | tf_op jit(solution)/shard_map/ppermute | solution.py:28
  204.1 0.8 copy-start.3
  204.9 0.8 copy-start.4
  214.5 0.8 copy-start.15

commit v2 on v1

--- a/solution.py
+++ b/solution.py
@@ -79,8 +79,17 @@
     outs = (o0, o1)
     tokens, width = x_ref.shape
     rows, part = o0.shape
-    for copy in fetch((x_hbm, gain_hbm, ids_hbm), (x_ref, gain_ref, ids_ref), sems):
-        copy.wait()
+    ids_copy, x_copy, gain_copy = fetch(
+        (ids_hbm, x_hbm, gain_hbm), (ids_ref, x_ref, gain_ref), sems
+    )
+    ids_copy.wait()
+    _, _, chosen, earlier, place = slot_tables(ids_ref[...], rows, tokens, per_chunk)
+    picks = [
+        jnp.logical_and(chosen, earlier == place + chunk * per_chunk).astype(f32).astype(bf16)
+        for chunk in range(len(outs))
+    ]
+    x_copy.wait()
+    gain_copy.wait()
     squares = jnp.zeros((tokens, 128), f32)
     for begin in range(0, width, 128):
         block = x_ref[:, begin : begin + 128].astype(f32)
@@ -89,10 +98,8 @@
     start = pl.multiple_of(tp_ref[0] * part, part)
     mine = x_ref[:, pl.ds(start, part)].astype(f32)
     normed = (mine * scale * gain_ref[:, pl.ds(start, part)]).astype(bf16)
-    _, _, chosen, earlier, place = slot_tables(ids_ref[...], rows, tokens, per_chunk)
-    for chunk, out in enumerate(outs):
-        pick = jnp.logical_and(chosen, earlier == place + chunk * per_chunk)
-        out[...] = dot(pick.astype(f32).astype(bf16), normed).astype(bf16)
+    for pick, out in zip(picks, outs):
+        out[...] = dot(pick, normed).astype(bf16)
 
 
 def route_kernel(per_chunk, ids_ref, weight_ref, high_ref, low_ref):
@@ -107,75 +114,90 @@
         low_ref[:, chunk * rows : (chunk + 1) * rows] = (weights - high.astype(f32)).astype(bf16)
 
 
-def expert_kernel(chunk, tp_ref, own, ahead, behind, *refs):
-    if chunk == 0:
-        across_in, *refs = refs
-    else:
-        top, bottom, *refs = refs
-    weights, outs, scratch = refs[:3], refs[3:-7], refs[-7:]
-    kept, (to_ahead, to_behind, across), sems = scratch[:3], scratch[3:6], scratch[6]
+def rows_of_blocks(tp, part, count):
+    return [pl.multiple_of(lax.rem(tp + k, count) * part, part) for k in (0, 1, count - 1, 2)]
+
+
+def expert_rows(at, blocks, starts, gate_ref, up_ref, down_ref, outs, arrive):
+    part = blocks[0].shape[1]
+    gate = None
+    up = None
+    for k, (x, start) in enumerate(zip(blocks, starts)):
+        arrive(k)
+        block = x[at, :]
+        g = dot(block, gate_ref[pl.ds(start, part), :])
+        u = dot(block, up_ref[pl.ds(start, part), :])
+        gate = g if gate is None else gate + g
+        up = u if up is None else up + u
+    hidden = (jax.nn.silu(gate) * up).astype(bf16)
+    arrive(len(blocks))
+    for out, start in zip(outs, starts):
+        out[at, :] = dot(hidden, down_ref[:, pl.ds(start, part)]).astype(bf16)
+
+
+def first_expert_kernel(
+    tp_ref, x0, x1, x2, x3, gate_hbm, up_hbm, down_hbm,
+    to_own, to_ahead, to_behind, across_top, across_bottom, gate_ref, up_ref, down_ref,
+    own, ahead, behind, across_in, across, sems,
+):
     rows, part = own.shape
     half = rows // 2
-    width = weights[0].shape[0]
-    count = width // part
-    tp = tp_ref[0]
-    starts = [
-        pl.multiple_of(lax.rem(tp + k, count) * part, part) for k in (0, 1, count - 1, 2)
-    ]
-    gate_ref, up_ref, down_ref = kept
+    blocks = (own, ahead, behind, across_in)
+    starts = rows_of_blocks(tp_ref[0], part, gate_ref.shape[0] // part)
     sources, targets = [], []
-    for start in starts:
-        for source, target in zip(weights[:2], kept[:2]):
-            sources.append(source.at[pl.ds(start, part), :])
-            targets.append(target.at[pl.ds(start, part), :])
-    copies = fetch(sources + [weights[2]], targets + [down_ref], sems)
-    if chunk == 0:
-        to_own, ahead_out, behind_out, across_top, across_bottom = outs
-        to_ahead, to_behind = ahead_out, behind_out
-        blocks = (own, ahead, behind, across_in)
-    else:
-        to_own, ahead_top, ahead_bottom, behind_top, behind_bottom, across_top, across_bottom = outs
-        across[:half, :] = top[...]
-        across[half:, :] = bottom[...]
-        blocks = (own, ahead, behind, across)
+    for hbm, block, start in zip((x0, x1, x2, x3), blocks, starts):
+        at = pl.ds(start, part)
+        sources += [hbm, gate_hbm.at[at, :], up_hbm.at[at, :]]
+        targets += [block, gate_ref.at[at, :], up_ref.at[at, :]]
+    depth = down_ref.shape[0] // 3
+    for k in range(3):
+        at = pl.ds(k * depth, depth)
+        sources.append(down_hbm.at[at, :])
+        targets.append(down_ref.at[at, :])
+    copies = fetch(sources, targets, sems)
+
+    def arrive(k):
+        for copy in copies[3 * k : 3 * k + 3]:
+            copy.wait()
+
+    outs = (to_own, to_ahead, to_behind, across)
+    expert_rows(pl.ds(0, half), blocks, starts, gate_ref, up_ref, down_ref, outs, arrive)
+    expert_rows(
+        pl.ds(half, half), blocks, starts, gate_ref, up_ref, down_ref, outs, lambda k: None
+    )
+    across_top[...] = across[:half, :]
+    across_bottom[...] = across[half:, :]
+
+
+def second_expert_kernel(
+    tp_ref, own, ahead, behind, top, bottom, gate_ref, up_ref, down_ref,
+    to_own, ahead_top, ahead_bottom, behind_top, behind_bottom, across_top, across_bottom,
+    across, to_ahead, to_behind,
+):
+    rows, part = own.shape
+    half = rows // 2
+    across[:half, :] = top[...]
+    across[half:, :] = bottom[...]
+    blocks = (own, ahead, behind, across)
+    starts = rows_of_blocks(tp_ref[0], part, gate_ref.shape[0] // part)
 
     def step(i, carry):
         at = pl.ds(pl.multiple_of(i * half, half), half)
-        gate = None
-        up = None
-        for k, (x, start) in enumerate(zip(blocks, starts)):
-
-            @pl.when(i == 0)
-            def _():
-                copies[2 * k].wait()
-                copies[2 * k + 1].wait()
-
-            block = x[at, :]
-            g = dot(block, gate_ref[pl.ds(start, part), :])
-            u = dot(block, up_ref[pl.ds(start, part), :])
-            gate = g if gate is None else gate + g
-            up = u if up is None else up + u
-        hidden = (jax.nn.silu(gate) * up).astype(bf16)
-
-        @pl.when(i == 0)
-        def _():
-            copies[-1].wait()
-
-        for out, start in zip((to_own, to_ahead, to_behind, across), starts):
-            out[at, :] = dot(hidden, down_ref[:, pl.ds(start, part)]).astype(bf16)
+        outs = (to_own, to_ahead, to_behind, across)
+        expert_rows(at, blocks, starts, gate_ref, up_ref, down_ref, outs, lambda k: None)
         return carry
 
     lax.fori_loop(0, 2, step, 0)
-    across_top[...] = across[:half, :]
-    across_bottom[...] = across[half:, :]
-    if chunk == 1:
-        ahead_top[...] = to_ahead[:half, :]
-        ahead_bottom[...] = to_ahead[half:, :]
-        behind_top[...] = to_behind[:half, :]
-        behind_bottom[...] = to_behind[half:, :]
-
-
-def fold_whole_kernel(ahead, top, behind, bottom, ahead_out, behind_out):
+    for source, upper, lower in (
+        (across, across_top, across_bottom),
+        (to_ahead, ahead_top, ahead_bottom),
+        (to_behind, behind_top, behind_bottom),
+    ):
+        upper[...] = source[:half, :]
+        lower[...] = source[half:, :]
+
+
+def fold_kernel(ahead, top, behind, bottom, ahead_out, behind_out):
     half = top.shape[0]
     ahead_out[:half, :] = (ahead[:half, :].astype(f32) + top[...].astype(f32)).astype(bf16)
     ahead_out[half:, :] = ahead[half:, :]
@@ -183,23 +205,24 @@
     behind_out[half:, :] = (behind[half:, :].astype(f32) + bottom[...].astype(f32)).astype(bf16)
 
 
-def total_whole_kernel(own, first, second, out):
-    out[...] = (own[...].astype(f32) + first[...].astype(f32) + second[...].astype(f32)).astype(bf16)
-
-
-def fold_kernel(a, b, c, d, ab, cd):
+def total_kernel(*refs):
+    out = refs[-1]
+    out[...] = sum(term[...].astype(f32) for term in refs[:-1]).astype(bf16)
+
+
+def total_halves_kernel(own, top0, top1, bottom0, bottom1, out, *scratch):
+    half = top0.shape[0]
+    copies = fetch((own, top0, bottom0, top1, bottom1), scratch[:5], scratch[5])
+    for copy in copies:
+        copy.wait()
+    own, top0, bottom0, top1, bottom1 = (ref[...].astype(f32) for ref in scratch[:5])
+    out[:half, :] = (own[:half, :] + top0 + top1).astype(bf16)
+    out[half:, :] = (own[half:, :] + bottom0 + bottom1).astype(bf16)
+
+
+def fold_halves_kernel(a, b, c, d, ab, cd):
     ab[...] = (a[...].astype(f32) + b[...].astype(f32)).astype(bf16)
     cd[...] = (c[...].astype(f32) + d[...].astype(f32)).astype(bf16)
-
-
-def total_kernel(own, top0, top1, bottom0, bottom1, out):
-    half = top0.shape[0]
-    out[:half, :] = (
-        own[:half, :].astype(f32) + top0[...].astype(f32) + top1[...].astype(f32)
-    ).astype(bf16)
-    out[half:, :] = (
-        own[half:, :].astype(f32) + bottom0[...].astype(f32) + bottom1[...].astype(f32)
-    ).astype(bf16)
 
 
 def conv_kernel_body(reach, halo, b0, b1, b2, b3, out_ref, wide, kept):
@@ -234,30 +257,30 @@
         out_ref[:, lanes] = jax.nn.silu(scaled).astype(bf16)
 
 
-def mix_kernel(core_ref, act, own, n1, n2, n3, far_ref, out_ref):
+def mix_kernel(core_ref, act, own, n1, n2, n3, f12, f3, out_ref):
     part = own.shape[0]
     columns = n1.shape[1]
     core = core_ref[0]
     near_at = pl.ds(pl.multiple_of(core * columns, columns), columns)
     far_at = pl.ds(pl.multiple_of((1 - core) * columns, columns), columns)
-    cut = lambda k: act[:, k * part : (k + 1) * part]
+    cut = lambda k, n=1: act[:, k * part : (k + n) * part]
     near = dot(cut(0), own[:, near_at]) + dot(cut(1), n1[...])
     near = near + dot(cut(2), n2[...]) + dot(cut(3), n3[...])
     out_ref[:, near_at] = near.astype(bf16)
-    far = dot(cut(0), own[:, far_at]) + dot(act[:, part:], far_ref[...])
+    far = dot(cut(0), own[:, far_at]) + dot(cut(1, 2), f12[...]) + dot(cut(3), f3[...])
     out_ref[:, far_at] = far.astype(bf16)
 
 
-def combine_kernel(high_ref, low_ref, a0_hbm, a1_hbm, out_ref, a0, a1, sems):
+def combine_kernel(high_hbm, low_hbm, a0_hbm, a1_hbm, out_ref, high_ref, low_ref, a0, a1, sems):
     rows = a0.shape[0]
-    copies = fetch((a0_hbm, a1_hbm), (a0, a1), sems)
-    total = None
-    for chunk, (copy, answers) in enumerate(zip(copies, (a0, a1))):
+    copies = fetch(
+        (high_hbm, a0_hbm, low_hbm, a1_hbm), (high_ref, a0, low_ref, a1), sems
+    )
+    for copy in copies[:3]:
         copy.wait()
-        cols = slice(chunk * rows, (chunk + 1) * rows)
-        for weights in (high_ref, low_ref):
-            term = dot(weights[:, cols], answers[...])
-            total = term if total is None else total + term
+    total = dot(high_ref[:, :rows], a0[...]) + dot(low_ref[:, :rows], a0[...])
+    copies[3].wait()
+    total = total + dot(high_ref[:, rows:], a1[...]) + dot(low_ref[:, rows:], a1[...])
     out_ref[...] = total.astype(bf16)
 
 
@@ -295,8 +318,10 @@
     halo = 32
     columns = out_weight.shape[1] // 2
     mine = lax.dynamic_slice_in_dim(out_weight, core * columns, columns, 1)
-    near = gather_direct(mine)
-    far = swap_cores(jnp.concatenate(near, axis=0))
+    near = [over_tp(mine, -1), over_tp(mine, 1)]
+    far = [swap_cores(jnp.concatenate(near, axis=0))]
+    near.append(over_tp(mine, 2))
+    far.append(swap_cores(near[2]))
     taps = jnp.concatenate([conv_kernel, ln_gain[None, :]], axis=0)
     taps = split_three(taps)
     gated = (glu_value.astype(f32) * jax.nn.sigmoid(glu_gate.astype(f32))).astype(bf16)
@@ -324,10 +349,10 @@
     return call(
         mix_kernel,
         shape(own, 2 * columns),
-        [SMEM] + [VMEM] * 6,
+        [SMEM] + [VMEM] * 7,
         2 * own * part * count * 2 * columns,
         8,
-    )(core.astype(jnp.int32).reshape(1), activated, out_weight, *near, far)
+    )(core.astype(jnp.int32).reshape(1), activated, out_weight, *near, *far)
 
 
 def expert_half(moe_input, moe_gain, gate_weight, up_weight, down_weight, expert_ids, route_weight):
@@ -370,56 +395,66 @@
     )(ids, route_weight.T)
     weights = (gate_weight[0], up_weight[0], down_weight[0])
     whole, halves = shape(rows, part), shape(half, part)
-
-    def run(chunk, outs, blocks):
-        return call(
-            functools.partial(expert_kernel, chunk),
-            outs,
-            [SMEM] + [VMEM] * len(blocks) + [ANY] * 3,
-            6 * rows * width * gate_weight.shape[2],
-            50,
-            [pltpu.VMEM(w.shape, bf16) for w in weights]
-            + [pltpu.VMEM((rows, part), bf16)] * 3
-            + [pltpu.SemaphoreType.DMA((2 * count + 1,))],
-        )(tp, *blocks, *weights)
-
-    def fold(kernel, kind, *terms):
-        return call(kernel, [kind] * 2, [VMEM] * 4, 10**8, 8)(*terms)
-
-    def total(kernel, *terms):
-        return call(kernel, whole, [VMEM] * len(terms), 10**8, 8)(*terms)
+    flops = 6 * rows * width * gate_weight.shape[2]
+    vmem_blocks = [pltpu.VMEM((rows, part), bf16)]
+
+    def total(*terms):
+        return call(total_kernel, whole, [VMEM] * len(terms), 10**8, 8)(*terms)
 
     arrived = exchange(sent[0])
     others = gather_direct(arrived)
-    own, ahead, behind, top, bottom = run(0, [whole] * 3 + [halves] * 2, (arrived, *others))
+    own, ahead, behind, top, bottom, *weights = call(
+        first_expert_kernel,
+        [whole] * 3 + [halves] * 2 + [shape(*w.shape) for w in weights],
+        [SMEM] + [ANY] * 7,
+        flops,
+        39,
+        vmem_blocks * 5 + [pltpu.SemaphoreType.DMA((3 * count + 3,))],
+    )(tp, arrived, *others, *weights)
     top = over_tp(top, 1)
     bottom = over_tp(bottom, -1)
-    ahead, behind = fold(fold_whole_kernel, whole, ahead, top, behind, bottom)
+    ahead, behind = call(fold_kernel, [whole] * 2, [VMEM] * 4, 10**8, 8)(ahead, top, behind, bottom)
     ahead = over_tp(ahead, 1)
     behind = over_tp(behind, -1)
-    answer = total(total_whole_kernel, own, ahead, behind)
+    answer = total(own, ahead, behind)
     answers = [exchange(answer)]
     arrived = exchange(sent[1])
     others = gather_relayed(arrived)
-    own, ahead0, ahead1, behind0, behind1, across0, across1 = run(
-        1, [whole] + [halves] * 6, (arrived, *others)
-    )
+    own, ahead0, ahead1, behind0, behind1, across0, across1 = call(
+        second_expert_kernel,
+        [whole] + [halves] * 6,
+        [SMEM] + [VMEM] * 8,
+        flops,
+        16,
+        vmem_blocks * 3,
+    )(tp, arrived, *others, *weights)
     across0 = over_tp(across0, 1)
     across1 = over_tp(across1, -1)
     bottom0 = over_tp(ahead1, 1)
     top0 = over_tp(behind0, -1)
-    ahead0, behind1 = fold(fold_kernel, halves, ahead0, across0, behind1, across1)
+    ahead0, behind1 = call(
+        fold_halves_kernel, [halves] * 2, [VMEM] * 4, 10**8, 8
+    )(ahead0, across0, behind1, across1)
     top1 = over_tp(ahead0, 1)
     bottom1 = over_tp(behind1, -1)
-    answer = total(total_kernel, own, top0, top1, bottom0, bottom1)
+    answer = call(
+        total_halves_kernel,
+        whole,
+        [ANY] * 5,
+        10**8,
+        56,
+        vmem_blocks + [pltpu.VMEM((half, part), bf16)] * 4 + [pltpu.SemaphoreType.DMA((5,))],
+    )(own, top0, top1, bottom0, bottom1)
     answers.append(exchange(answer))
     return call(
         combine_kernel,
         shape(tokens, part),
-        [VMEM, VMEM, ANY, ANY],
+        [ANY] * 4,
         4 * tokens * rows * part,
         56,
-        [pltpu.VMEM((rows, part), bf16)] * 2 + [pltpu.SemaphoreType.DMA((2,))],
+        [pltpu.VMEM((tokens, experts * capacity), bf16)] * 2
+        + vmem_blocks * 2
+        + [pltpu.SemaphoreType.DMA((4,))],
     )(high, low, *answers)
 
 

time: 220 us -> 217 us (0.986)
  waiting for transfers between devices: 83.5 us -> 91.3 us
  local copies, waits for them, and re-layouts: 11 us -> 3.53 us
  Pallas kernels: 33.4 us -> 27.8 us
  starting transfers between devices: 59.6 us -> 62 us
    all_to_all x3, waiting for transfers between devices: 0.01 us -> 14.3 us  [exchange(): moved = lax.all_to_all(value, 'ep', split_axis=0, concat_axis=0, tiled=True)]
    unnamed x40 -> x28, local copies, waits for them, and re-layouts: 10.1 us -> 2.65 us
    pallas_call x8, Pallas kernels: 27.9 us -> 22.4 us  [the longest x1 7.87 us: expert_half(): call(first_expert_kernel, [whole] * 3 + [halves] * 2 + [shape(*w.shape) f...]
    ppermute x23, waiting for transfers between devices: 72 us -> 67.3 us  [over_tp(): lax.ppermute(value, 'tp', [(i, (i + by) % count) for i in range(count)])]
    ppermute x23, starting transfers between devices: 30.5 us -> 35.2 us  [over_tp(): lax.ppermute(value, 'tp', [(i, (i + by) % count) for i in range(count)])]
    all_to_all x3, starting transfers between devices: 27.1 us -> 23.2 us  [exchange(): moved = lax.all_to_all(value, 'ep', split_axis=0, concat_axis=0, tiled=True)]
  transfers between devices with their start and end apart: 28 -> 29, of which waited for: 14 -> 13; matrix products, arithmetic and copies ran while one was open for 2% -> 2% of each run, Pallas kernels for 12% -> 7%
where the time goes in v2:
time: 217 us; the launch traced here: 216 us
  waiting for transfers between devices  91.3 us (42%)
  starting transfers between devices  62 us (29%)
  blocking collectives  28 us (13%)
  Pallas kernels  27.8 us (13%)
  local copies, waits for them, and re-layouts  3.53 us (2%)
  other arithmetic  2.4 us (1%)
    ppermute x23, waiting for transfers between devices, over_tp(): lax.ppermute(value, 'tp', [(i, (i + by) % count) for i in range(count)])  67.3 us
    ppermute x23, starting transfers between devices, over_tp(): lax.ppermute(value, 'tp', [(i, (i + by) % count) for i in range(count)])  35.2 us
    all_to_all x1, blocking collectives, exchange(): moved = lax.all_to_all(value, 'ep', split_axis=0, concat_axis=0, tiled=True)  28 us
    all_to_all x3, starting transfers between devices, exchange(): moved = lax.all_to_all(value, 'ep', split_axis=0, concat_axis=0, tiled=True)  23.2 us
    all_to_all x3, waiting for transfers between devices, exchange(): moved = lax.all_to_all(value, 'ep', split_axis=0, concat_axis=0, tiled=True)  14.3 us
    ppermute x1, waiting for transfers between devices, from_behind(): return lax.ppermute(value, axis, [(i, i + by) for i in range(count - by)])  9.79 us
    pallas_call x1, Pallas kernels, expert_half(): call(first_expert_kernel, [whole] * 3 + [halves] * 2 + [shape(*w.shape) f...  7.87 us
    pallas_call x1, Pallas kernels, expert_half(): call(second_expert_kernel, [whole] + [halves] * 6, [SMEM] + [VMEM] * 8, f...  5.37 us
  transfers between devices with their start and end apart: 29, of which 13 were waited for; matrix products, arithmetic and copies ran while one was open for 2% of the time, Pallas kernels for 7%

profile of v2, /device:TPU:96, one launch (start us, length us, event | category | flops | bytes accessed | tf_op | source)
XLA Modules:
  0.0 216.3 jit_solution(564324508960542613)
XLA Ops:
  0.6 2.8 %shard_map.134 = (bf16[512,512]{1,0:T(8,128)(2,1)}, bf16[512,512]{1,0:T(8,128)(2,1)}) custom-call(s32[1]{0:T(128)} %bitcast.4.tp_ref, bf16[256,2048]{1,0:T(8,128)(2,1)} %x_hbm.1, f32[1,2048]{1,0:T(1,128)} %bitcast.30, s32[2,256]{1,0:T(2,128)} %bitcast.24), custom_call_target="tpu_custom_call" | custom-call | flops 268435456 | bytes 1048576 | tf_op jit(solution)/shard_map/pallas_call | solution.py:376
  3.5 28.0 %all_to_all.20 = bf16[64,8,512]{2,1,0:T(8,128)(2,1)S(1)} all-to-all(bf16[64,8,512]{2,1,0:T(8,128)(2,1)} %bitcast.29), channel_id=1, replica_groups=mesh['ep'=64,'tp'=4] {'ep'}, dimensions={0} | all-to-all | bytes 1048576 | tf_op jit(solution)/shard_map/all_to_all | solution.py:373
  31.4 6.3 %all-to-all-start = ((bf16[64,8,512]{2,1,0:T(8,128)(2,1)}), bf16[64,8,512]{2,1,0:T(8,128)(2,1)S(1)}, u32[]{:S(2)}, u32[]{:S(2)}) async-start(bf16[64,8,512]{2,1,0:T(8,128)(2,1)} %bitcast.28), calls=%async_computation | async-start | bytes 1048576 | tf_op jit(solution)/shard_map/all_to_all | solution.py:373
  37.7 2.8 %collective-permute-start.16 = (bf16[512,512]{1,0:T(8,128)(2,1)S(1)}, bf16[512,512]{1,0:T(8,128)(2,1)S(1)}, u32[]{:S(2)}, u32[]{:S(2)}) collective-permute-start(bf16[512,512]{1,0:T(8,128)(2,1)S(1)} %bitcast.17), channel_id=1, source_target_pairs={{0,3},{1,0},{2,1},{3,2},{4,7},{5,4},{6,5},{7,6},{8,11},{9,8},{10,9... | collective-permute-start | bytes 1572872 | tf_op jit(solution)/shard_map/ppermute | solution.py:28
  40.6 14.3 %all-to-all-done = bf16[64,8,512]{2,1,0:T(8,128)(2,1)S(1)} async-done(((bf16[64,8,512]{2,1,0:T(8,128)(2,1)}), bf16[64,8,512]{2,1,0:T(8,128)(2,1)S(1)}, u32[]{:S(2)}, u32[]{:S(2)}) %all-to-all-start) | async-done | bytes 524320 | tf_op jit(solution)/shard_map/all_to_all | solution.py:373
  54.8 2.8 %collective-permute-start.9 = (bf16[512,512]{1,0:T(8,128)(2,1)S(1)}, bf16[512,512]{1,0:T(8,128)(2,1)S(1)}, u32[]{:S(2)}, u32[]{:S(2)}) collective-permute-start(bf16[512,512]{1,0:T(8,128)(2,1)S(1)} %bitcast.20), channel_id=1, source_target_pairs={{0,3},{1,0},{2,1},{3,2},{4,7},{5,4},{6,5},{7,6},{8,11},{9,8},{10,9... | collective-permute-start | bytes 1572872 | tf_op jit(solution)/shard_map/ppermute | solution.py:28
  57.6 2.3 %collective-permute-start.11 = (bf16[512,512]{1,0:T(8,128)(2,1)S(1)}, bf16[512,512]{1,0:T(8,128)(2,1)S(1)}, u32[]{:S(2)}, u32[]{:S(2)}) collective-permute-start(bf16[512,512]{1,0:T(8,128)(2,1)S(1)} %bitcast.22), channel_id=1, source_target_pairs={{0,2},{1,3},{2,0},{3,1},{4,6},{5,7},{6,4},{7,5},{8,10},{9,11},{10,... | collective-permute-start | bytes 1572872 | tf_op jit(solution)/shard_map/ppermute | solution.py:28
  59.9 1.2 collective-permute-start.18
  61.1 1.1 collective-permute-start.19
  62.3 18.7 %collective-permute-done.9.x1 = bf16[512,512]{1,0:T(8,128)(2,1)S(1)} collective-permute-done((bf16[512,512]{1,0:T(8,128)(2,1)S(1)}, bf16[512,512]{1,0:T(8,128)(2,1)S(1)}, u32[]{:S(2)}, u32[]{:S(2)}) %collective-permute-start.9) | collective-permute-done | bytes 524320 | tf_op jit(solution)/shard_map/ppermute | solution.py:28
  81.0 3.8 %collective-permute-done.10.x2 = bf16[512,512]{1,0:T(8,128)(2,1)S(1)} collective-permute-done((bf16[512,512]{1,0:T(8,128)(2,1)S(1)}, bf16[512,512]{1,0:T(8,128)(2,1)S(1)}, u32[]{:S(2)}, u32[]{:S(2)}) %collective-permute-start.10) | collective-permute-done | bytes 524320 | tf_op jit(solution)/shard_map/ppermute | solution.py:28
  84.8 7.9 %shard_map.135 = (bf16[512,512]{1,0:T(8,128)(2,1)S(1)}, bf16[512,512]{1,0:T(8,128)(2,1)S(1)}, bf16[512,512]{1,0:T(8,128)(2,1)S(1)}, bf16[256,512]{1,0:T(8,128)(2...) custom-call(s32[1]{0:T(128)} %bitcast.4.tp_ref, ...), custom_call_target="tpu_custom_call" | custom-call | flops 4831838208 | bytes 1048576 | tf_op jit(solution)/shard_map/pallas_call | solution.py:406
  92.7 5.4 %shard_map.138 = (bf16[512,512]{1,0:T(8,128)(2,1)S(1)}, bf16[256,512]{1,0:T(8,128)(2,1)S(1)}, bf16[256,512]{1,0:T(8,128)(2,1)S(1)}, bf16[256,512]{1,0:T(8,128)(2...) custom-call(s32[1]{0:T(128)} %bitcast.4.tp_ref, ...), custom_call_target="tpu_custom_call" | custom-call | flops 4831838208 | bytes 1048576 | tf_op jit(solution)/shard_map/pallas_call | solution.py:423
  98.1 0.8 copy-done.3
  98.9 3.2 %collective-permute-start.22 = (bf16[256,512]{1,0:T(8,128)(2,1)S(1)}, bf16[256,512]{1,0:T(8,128)(2,1)S(1)}, u32[]{:S(2)}, u32[]{:S(2)}) collective-permute-start(bf16[256,512]{1,0:T(8,128)(2,1)S(1)} %get-tuple-element.44), channel_id=1, source_target_pairs={{0,3},{1,0},{2,1},{3,2},{4,7},{5,4},{6,5},{7,6},{8,11},{9,8},{10,9... | collective-permute-start | bytes 786440 | tf_op jit(solution)/shard_map/ppermute | solution.py:28
  102.2 2.0 collective-permute-start.24
  104.2 4.9 %collective-permute-done.21.b = bf16[256,512]{1,0:T(8,128)(2,1)S(1)} collective-permute-done((bf16[256,512]{1,0:T(8,128)(2,1)S(1)}, bf16[256,512]{1,0:T(8,128)(2,1)S(1)}, u32[]{:S(2)}, u32[]{:S(2)}) %collective-permute-start.21) | collective-permute-done | bytes 262176 | tf_op jit(solution)/shard_map/ppermute | solution.py:28
  109.3 3.5 %collective-permute-start.25 = (bf16[256,512]{1,0:T(8,128)(2,1)S(1)}, bf16[256,512]{1,0:T(8,128)(2,1)S(1)}, u32[]{:S(2)}, u32[]{:S(2)}) collective-permute-start(bf16[256,512]{1,0:T(8,128)(2,1)S(1)} %get-tuple-element.47), channel_id=1, source_target_pairs={{0,3},{1,0},{2,1},{3,2},{4,7},{5,4},{6,5},{7,6},{8,11},{9,8},{10,9... | collective-permute-start | bytes 786440 | tf_op jit(solution)/shard_map/ppermute | solution.py:28
  112.8 4.2 %collective-permute-done.23.top1 = bf16[256,512]{1,0:T(8,128)(2,1)S(1)} collective-permute-done((bf16[256,512]{1,0:T(8,128)(2,1)S(1)}, bf16[256,512]{1,0:T(8,128)(2,1)S(1)}, u32[]{:S(2)}, u32[]{:S(2)}) %collective-permute-start.23) | collective-permute-done | bytes 262176 | tf_op jit(solution)/shard_map/ppermute | solution.py:28
  117.1 0.7 copy-done.10
  117.9 2.4 %shard_map.140 = bf16[512,512]{1,0:T(8,128)(2,1)} custom-call(bf16[512,512]{1,0:T(8,128)(2,1)} %copy-done.3, bf16[256,512]{1,0:T(8,128)(2,1)} %copy-done.8, bf16[256,512]{1,0:T(8,128)(2,1)} %copy-done.10, bf16[256,512]{1,0:T(8,128)(2,1)} %copy-done.9, bf16[256,512]{1,0:T(8,128)(2,1)} %copy-done.11), custom_call_target="tpu_custom_call" | custom-call | flops 100000000 | bytes 1048576 | tf_op jit(solution)/shard_map/pallas_call | solution.py:440
  120.2 6.4 %all-to-all-start.3 = ((bf16[64,8,512]{2,1,0:T(8,128)(2,1)}), bf16[64,8,512]{2,1,0:T(8,128)(2,1)}, u32[]{:S(2)}, u32[]{:S(2)}) async-start(bf16[64,8,512]{2,1,0:T(8,128)(2,1)} %bitcast.27), calls=%async_computation.3 | async-start | bytes 1048576 | tf_op jit(solution)/shard_map/all_to_all | solution.py:373
  126.7 1.4 collective-permute-start.12
  128.1 2.1 collective-permute-start.13
  130.2 0.8 constant_dynamic-slice_fusion
  131.1 1.9 collective-permute-start.4
  133.1 4.5 %collective-permute-done.12.top = bf16[256,512]{1,0:T(8,128)(2,1)S(1)} collective-permute-done((bf16[256,512]{1,0:T(8,128)(2,1)}, bf16[256,512]{1,0:T(8,128)(2,1)S(1)}, u32[]{:S(2)}, u32[]{:S(2)}) %collective-permute-start.12) | collective-permute-done | bytes 262176 | tf_op jit(solution)/shard_map/ppermute | solution.py:28
  137.7 1.8 collective-permute-start.14
  139.6 1.5 collective-permute-start.15
  141.1 2.0 collective-permute-start.6
  143.0 5.5 %collective-permute-done.4.n1 = bf16[256,1024]{1,0:T(8,128)(2,1)S(1)} collective-permute-done((bf16[256,1024]{1,0:T(8,128)(2,1)}, bf16[256,1024]{1,0:T(8,128)(2,1)S(1)}, u32[]{:S(2)}, u32[]{:S(2)}) %collective-permute-start.4) | collective-permute-done | bytes 524320 | tf_op jit(solution)/shard_map/ppermute | solution.py:28
  148.5 0.7 collective-permute-done.5.n2
  149.2 1.1 pad_maximum_fusion
  150.3 9.1 %collective-permute-done.14.refs_1_ = bf16[512,512]{1,0:T(8,128)(2,1)S(1)} collective-permute-done((bf16[512,512]{1,0:T(8,128)(2,1)S(1)}, bf16[512,512]{1,0:T(8,128)(2,1)S(1)}, u32[]{:S(2)}, u32[]{:S(2)}) %collective-permute-start.14) | collective-permute-done | bytes 524320 | tf_op jit(solution)/shard_map/ppermute | solution.py:28
  159.4 10.4 %collective-permute-done.15.refs_2_ = bf16[512,512]{1,0:T(8,128)(2,1)S(1)} collective-permute-done((bf16[512,512]{1,0:T(8,128)(2,1)S(1)}, bf16[512,512]{1,0:T(8,128)(2,1)S(1)}, u32[]{:S(2)}, u32[]{:S(2)}) %collective-permute-start.15) | collective-permute-done | bytes 524320 | tf_op jit(solution)/shard_map/ppermute | solution.py:28
  169.8 1.0 copy-done.2
  170.8 1.0 shard_map.137
  171.8 10.5 %all-to-all-start.1 = ((bf16[64,8,512]{2,1,0:T(8,128)(2,1)}), bf16[64,8,512]{2,1,0:T(8,128)(2,1)}, u32[]{:S(2)}, u32[]{:S(2)}) async-start(bf16[64,8,512]{2,1,0:T(8,128)(2,1)} %bitcast.11), calls=%async_computation.1 | async-start | bytes 1048576 | tf_op jit(solution)/shard_map/all_to_all | solution.py:373
  182.3 1.2 multiply_convert_fusion
  183.5 2.0 collective-permute-start
  185.6 1.6 collective-permute-start.8
  187.2 9.8 %collective-permute-done = bf16[32,256]{1,0:T(8,128)(2,1)S(1)} collective-permute-done((bf16[32,256]{1,0:T(8,128)(2,1)S(1)}, bf16[32,256]{1,0:T(8,128)(2,1)S(1)}, u32[]{:S(2)}, u32[]{:S(2)}) %collective-permute-start) | collective-permute-done | bytes 16416 | tf_op jit(solution)/shard_map/ppermute | solution.py:33
  197.1 3.7 %collective-permute-start.1 = (bf16[256,256]{1,0:T(8,128)(2,1)S(1)}, bf16[256,256]{1,0:T(8,128)(2,1)S(1)}, u32[]{:S(2)}, u32[]{:S(2)}) collective-permute-start(bf16[256,256]{1,0:T(8,128)(2,1)S(1)} %get-tuple-element.53), channel_id=1, source_target_pairs={{0,3},{1,0},{2,1},{3,2},{4,7},{5,4},{6,5},{7,6},{8,11},{9,8},{10,9... | collective-permute-start | bytes 393224 | tf_op jit(solution)/shard_map/ppermute | solution.py:28
  200.9 1.6 collective-permute-start.3
  203.4 5.1 %collective-permute-done.2.b2 = bf16[256,256]{1,0:T(8,128)(2,1)S(1)} collective-permute-done((bf16[256,256]{1,0:T(8,128)(2,1)S(1)}, bf16[256,256]{1,0:T(8,128)(2,1)S(1)}, u32[]{:S(2)}, u32[]{:S(2)}) %collective-permute-start.2) | collective-permute-done | bytes 131104 | tf_op jit(solution)/shard_map/ppermute | solution.py:28
  208.4 2.0 shard_map.131.act
  210.5 2.7 %shard_map.132 = bf16[128,2048]{1,0:T(8,128)(2,1)} custom-call(s32[1]{0:T(128)} %bitcast.core_ref, bf16[128,1024]{1,0:T(8,128)(2,1)S(1)} %shard_map.131.act, bf16[256,2048]{1,0:T(8,128)(2,1)S(1)} %copy-done, bf16[256,1024]{1,0:T(8,128)(2,1)S(1)} %collective-permute-done.4.n1, bf16[256,1024]{1,0:T(8,128)(2,1)S(1)} %collective-permute-done.5.n2, ...), custom_call_target="tpu_custom_call" | custom-call | flops 536870912 | bytes 1048576 | tf_op jit(solution)/shard_map/pallas_call | solution.py:349
  213.2 2.9 %shard_map.141 = bf16[256,512]{1,0:T(8,128)(2,1)} custom-call(bf16[256,1024]{1,0:T(8,128)(2,1)} %copy-done.4, bf16[256,1024]{1,0:T(8,128)(2,1)} %copy-done.5, bf16[512,512]{1,0:T(8,128)(2,1)} %bitcast.12.a0_hbm, bf16[512,512]{1,0:T(8,128)(2,1)} %bitcast.16.a1_hbm), custom_call_target="tpu_custom_call" | custom-call | flops 268435456 | bytes 1048576 | tf_op jit(solution)/shard_map/pallas_call | solution.py:449
  (60 shorter events, 1.8 us)
Async XLA Ops:
  31.4 23.4 %all-to-all-start = ((bf16[64,8,512]{2,1,0:T(8,128)(2,1)}), bf16[64,8,512]{2,1,0:T(8,128)(2,1)S(1)}, u32[]{:S(2)}, u32[]{:S(2)}) async-start(bf16[64,8,512]{2,1,0:T(8,128)(2,1)} %bitcast.28), calls=%async_computation | async-start | bytes 1048576 | tf_op jit(solution)/shard_map/all_to_all | solution.py:373
  37.7 22.1 %collective-permute-start.16 = (bf16[512,512]{1,0:T(8,128)(2,1)S(1)}, bf16[512,512]{1,0:T(8,128)(2,1)S(1)}, u32[]{:S(2)}, u32[]{:S(2)}) collective-permute-start(bf16[512,512]{1,0:T(8,128)(2,1)S(1)} %bitcast.17), channel_id=1, source_target_pairs={{0,3},{1,0},{2,1},{3,2},{4,7},{5,4},{6,5},{7,6},{8,11},{9,8},{10,9... | collective-permute-start | bytes 1572872 | tf_op jit(solution)/shard_map/ppermute | solution.py:28
  40.6 20.5 %collective-permute-start.17 = (bf16[512,512]{1,0:T(8,128)(2,1)S(1)}, bf16[512,512]{1,0:T(8,128)(2,1)S(1)}, u32[]{:S(2)}, u32[]{:S(2)}) collective-permute-start(bf16[512,512]{1,0:T(8,128)(2,1)S(1)} %bitcast.18), channel_id=1, source_target_pairs={{0,1},{1,2},{2,3},{3,0},{4,5},{5,6},{6,7},{7,4},{8,9},{9,10},{10,1... | collective-permute-start | bytes 1572872 | tf_op jit(solution)/shard_map/ppermute | solution.py:28
  54.8 26.2 %collective-permute-start.9 = (bf16[512,512]{1,0:T(8,128)(2,1)S(1)}, bf16[512,512]{1,0:T(8,128)(2,1)S(1)}, u32[]{:S(2)}, u32[]{:S(2)}) collective-permute-start(bf16[512,512]{1,0:T(8,128)(2,1)S(1)} %bitcast.20), channel_id=1, source_target_pairs={{0,3},{1,0},{2,1},{3,2},{4,7},{5,4},{6,5},{7,6},{8,11},{9,8},{10,9... | collective-permute-start | bytes 1572872 | tf_op jit(solution)/shard_map/ppermute | solution.py:28
  57.6 27.2 %collective-permute-start.10 = (bf16[512,512]{1,0:T(8,128)(2,1)S(1)}, bf16[512,512]{1,0:T(8,128)(2,1)S(1)}, u32[]{:S(2)}, u32[]{:S(2)}) collective-permute-start(bf16[512,512]{1,0:T(8,128)(2,1)S(1)} %bitcast.21), channel_id=1, source_target_pairs={{0,1},{1,2},{2,3},{3,0},{4,5},{5,6},{6,7},{7,4},{8,9},{9,10},{10,1... | collective-permute-start | bytes 1572872 | tf_op jit(solution)/shard_map/ppermute | solution.py:28
  57.6 27.2 %collective-permute-start.11 = (bf16[512,512]{1,0:T(8,128)(2,1)S(1)}, bf16[512,512]{1,0:T(8,128)(2,1)S(1)}, u32[]{:S(2)}, u32[]{:S(2)}) collective-permute-start(bf16[512,512]{1,0:T(8,128)(2,1)S(1)} %bitcast.22), channel_id=1, source_target_pairs={{0,2},{1,3},{2,0},{3,1},{4,6},{5,7},{6,4},{7,5},{8,10},{9,11},{10,... | collective-permute-start | bytes 1572872 | tf_op jit(solution)/shard_map/ppermute | solution.py:28
  59.9 32.8 %collective-permute-start.18 = (bf16[256,512]{1,0:T(8,128)(2,1)S(1)}, bf16[256,512]{1,0:T(8,128)(2,1)S(1)}, u32[]{:S(2)}, u32[]{:S(2)}) collective-permute-start(bf16[256,512]{1,0:T(8,128)(2,1)S(1)} %slice.13), channel_id=1, source_target_pairs={{0,3},{1,0},{2,1},{3,2},{4,7},{5,4},{6,5},{7,6},{8,11},{9,8},{10,9... | collective-permute-start | bytes 786440 | tf_op jit(solution)/shard_map/ppermute | solution.py:28
  61.1 31.6 %collective-permute-start.19 = (bf16[256,512]{1,0:T(8,128)(2,1)S(1)}, bf16[256,512]{1,0:T(8,128)(2,1)S(1)}, u32[]{:S(2)}, u32[]{:S(2)}) collective-permute-start(bf16[256,512]{1,0:T(8,128)(2,1)S(1)} %slice.14), channel_id=1, source_target_pairs={{0,1},{1,2},{2,3},{3,0},{4,5},{5,6},{6,7},{7,4},{8,9},{9,10},{10,1... | collective-permute-start | bytes 786440 | tf_op jit(solution)/shard_map/ppermute | solution.py:28
  92.7 5.4 %copy-start.1 = (bf16[512,512]{1,0:T(8,128)(2,1)}, bf16[512,512]{1,0:T(8,128)(2,1)S(1)}, u32[]{:S(2)}) copy-start(bf16[512,512]{1,0:T(8,128)(2,1)S(1)} %get-tuple-element.28.refs_0_) | copy-start | bytes 1572868
  98.1 0.8 copy-start.3
  98.9 31.3 %copy-start = (bf16[256,2048]{1,0:T(8,128)(2,1)S(1)}, bf16[256,2048]{1,0:T(8,128)(2,1)}, u32[]{:S(2)}) copy-start(bf16[256,2048]{1,0:T(8,128)(2,1)} %own.1) | copy-start | bytes 3145732
  98.9 10.1 %collective-permute-start.21 = (bf16[256,512]{1,0:T(8,128)(2,1)S(1)}, bf16[256,512]{1,0:T(8,128)(2,1)S(1)}, u32[]{:S(2)}, u32[]{:S(2)}) collective-permute-start(bf16[256,512]{1,0:T(8,128)(2,1)S(1)} %get-tuple-element.42), channel_id=1, source_target_pairs={{0,1},{1,2},{2,3},{3,0},{4,5},{5,6},{6,7},{7,4},{8,9},{9,10},{10,1... | collective-permute-start | bytes 786440 | tf_op jit(solution)/shard_map/ppermute | solution.py:28
  98.9 10.1 %collective-permute-start.22 = (bf16[256,512]{1,0:T(8,128)(2,1)S(1)}, bf16[256,512]{1,0:T(8,128)(2,1)S(1)}, u32[]{:S(2)}, u32[]{:S(2)}) collective-permute-start(bf16[256,512]{1,0:T(8,128)(2,1)S(1)} %get-tuple-element.44), channel_id=1, source_target_pairs={{0,3},{1,0},{2,1},{3,2},{4,7},{5,4},{6,5},{7,6},{8,11},{9,8},{10,9... | collective-permute-start | bytes 786440 | tf_op jit(solution)/shard_map/ppermute | solution.py:28
  102.2 10.6 %collective-permute-start.20 = (bf16[256,512]{1,0:T(8,128)(2,1)S(1)}, bf16[256,512]{1,0:T(8,128)(2,1)S(1)}, u32[]{:S(2)}, u32[]{:S(2)}) collective-permute-start(bf16[256,512]{1,0:T(8,128)(2,1)S(1)} %get-tuple-element.40), channel_id=1, source_target_pairs={{0,3},{1,0},{2,1},{3,2},{4,7},{5,4},{6,5},{7,6},{8,11},{9,8},{10,9... | collective-permute-start | bytes 786440 | tf_op jit(solution)/shard_map/ppermute | solution.py:28
  102.2 10.6 %collective-permute-start.24 = (bf16[256,512]{1,0:T(8,128)(2,1)S(1)}, bf16[256,512]{1,0:T(8,128)(2,1)S(1)}, u32[]{:S(2)}, u32[]{:S(2)}) collective-permute-start(bf16[256,512]{1,0:T(8,128)(2,1)S(1)} %get-tuple-element.46), channel_id=1, source_target_pairs={{0,1},{1,2},{2,3},{3,0},{4,5},{5,6},{6,7},{7,4},{8,9},{9,10},{10,1... | collective-permute-start | bytes 786440 | tf_op jit(solution)/shard_map/ppermute | solution.py:28
  109.2 7.9 %collective-permute-start.23 = (bf16[256,512]{1,0:T(8,128)(2,1)S(1)}, bf16[256,512]{1,0:T(8,128)(2,1)S(1)}, u32[]{:S(2)}, u32[]{:S(2)}) collective-permute-start(bf16[256,512]{1,0:T(8,128)(2,1)S(1)} %get-tuple-element.45), channel_id=1, source_target_pairs={{0,1},{1,2},{2,3},{3,0},{4,5},{5,6},{6,7},{7,4},{8,9},{9,10},{10,1... | collective-permute-start | bytes 786440 | tf_op jit(solution)/shard_map/ppermute | solution.py:28
  109.3 7.8 %collective-permute-start.25 = (bf16[256,512]{1,0:T(8,128)(2,1)S(1)}, bf16[256,512]{1,0:T(8,128)(2,1)S(1)}, u32[]{:S(2)}, u32[]{:S(2)}) collective-permute-start(bf16[256,512]{1,0:T(8,128)(2,1)S(1)} %get-tuple-element.47), channel_id=1, source_target_pairs={{0,3},{1,0},{2,1},{3,2},{4,7},{5,4},{6,5},{7,6},{8,11},{9,8},{10,9... | collective-permute-start | bytes 786440 | tf_op jit(solution)/shard_map/ppermute | solution.py:28
  112.8 4.3 %copy-start.8 = (bf16[256,512]{1,0:T(8,128)(2,1)}, bf16[256,512]{1,0:T(8,128)(2,1)S(1)}, u32[]{:S(2)}) copy-start(bf16[256,512]{1,0:T(8,128)(2,1)S(1)} %collective-permute-done.20.top0) | copy-start | bytes 786436
  112.8 4.3 %copy-start.9 = (bf16[256,512]{1,0:T(8,128)(2,1)}, bf16[256,512]{1,0:T(8,128)(2,1)S(1)}, u32[]{:S(2)}) copy-start(bf16[256,512]{1,0:T(8,128)(2,1)S(1)} %collective-permute-done.24.bottom0) | copy-start | bytes 786436
  117.1 0.7 copy-start.10
  117.1 0.8 copy-start.11
  120.2 51.6 %all-to-all-start.3 = ((bf16[64,8,512]{2,1,0:T(8,128)(2,1)}), bf16[64,8,512]{2,1,0:T(8,128)(2,1)}, u32[]{:S(2)}, u32[]{:S(2)}) async-start(bf16[64,8,512]{2,1,0:T(8,128)(2,1)} %bitcast.27), calls=%async_computation.3 | async-start | bytes 1048576 | tf_op jit(solution)/shard_map/all_to_all | solution.py:373
  126.7 10.9 %collective-permute-start.12 = (bf16[256,512]{1,0:T(8,128)(2,1)}, bf16[256,512]{1,0:T(8,128)(2,1)S(1)}, u32[]{:S(2)}, u32[]{:S(2)}) collective-permute-start(bf16[256,512]{1,0:T(8,128)(2,1)} %get-tuple-element.30), channel_id=1, source_target_pairs={{0,1},{1,2},{2,3},{3,0},{4,5},{5,6},{6,7},{7,4},{8,9},{9,10},{10,1... | collective-permute-start | bytes 786440 | tf_op jit(solution)/shard_map/ppermute | solution.py:28
  128.1 9.5 %collective-permute-start.13 = (bf16[256,512]{1,0:T(8,128)(2,1)S(1)}, bf16[256,512]{1,0:T(8,128)(2,1)S(1)}, u32[]{:S(2)}, u32[]{:S(2)}) collective-permute-start(bf16[256,512]{1,0:T(8,128)(2,1)S(1)} %get-tuple-element.32), channel_id=1, source_target_pairs={{0,3},{1,0},{2,1},{3,2},{4,7},{5,4},{6,5},{7,6},{8,11},{9,8},{10,9... | collective-permute-start | bytes 786440 | tf_op jit(solution)/shard_map/ppermute | solution.py:28
  131.1 17.5 %collective-permute-start.4 = (bf16[256,1024]{1,0:T(8,128)(2,1)}, bf16[256,1024]{1,0:T(8,128)(2,1)S(1)}, u32[]{:S(2)}, u32[]{:S(2)}) collective-permute-start(bf16[256,1024]{1,0:T(8,128)(2,1)} %constant_dynamic-slice_fusion), channel_id=1, source_target_pairs={{0,3},{1,0},{2,1},{3,2},{4,7},{5,4},{6,5},{7,6},{8,11},{9,8},{10,9... | collective-permute-start | bytes 1572872 | tf_op jit(solution)/shard_map/ppermute | solution.py:28
  133.0 16.2 %collective-permute-start.5 = (bf16[256,1024]{1,0:T(8,128)(2,1)}, bf16[256,1024]{1,0:T(8,128)(2,1)S(1)}, u32[]{:S(2)}, u32[]{:S(2)}) collective-permute-start(bf16[256,1024]{1,0:T(8,128)(2,1)} %constant_dynamic-slice_fusion), channel_id=1, source_target_pairs={{0,1},{1,2},{2,3},{3,0},{4,5},{5,6},{6,7},{7,4},{8,9},{9,10},{10,1... | collective-permute-start | bytes 1572872 | tf_op jit(solution)/shard_map/ppermute | solution.py:28
  137.7 47.8 %copy-start.12 = (f32[31,256]{1,0:T(8,128)S(1)}, f32[31,256]{1,0:T(8,128)}, u32[]{:S(2)}) copy-start(f32[31,256]{1,0:T(8,128)} %param.14) | copy-start | bytes 95236
  137.7 47.8 %copy-start.13 = (f32[256]{0:T(256)S(1)}, f32[256]{0:T(256)}, u32[]{:S(2)}) copy-start(f32[256]{0:T(256)} %param.15) | copy-start | bytes 3076
  137.7 21.6 %collective-permute-start.14 = (bf16[512,512]{1,0:T(8,128)(2,1)S(1)}, bf16[512,512]{1,0:T(8,128)(2,1)S(1)}, u32[]{:S(2)}, u32[]{:S(2)}) collective-permute-start(bf16[512,512]{1,0:T(8,128)(2,1)S(1)} %get-tuple-element.33), channel_id=1, source_target_pairs={{0,1},{1,2},{2,3},{3,0},{4,5},{5,6},{6,7},{7,4},{8,9},{9,10},{10,1... | collective-permute-start | bytes 1572872 | tf_op jit(solution)/shard_map/ppermute | solution.py:28
  139.6 30.2 %collective-permute-start.15 = (bf16[512,512]{1,0:T(8,128)(2,1)S(1)}, bf16[512,512]{1,0:T(8,128)(2,1)S(1)}, u32[]{:S(2)}, u32[]{:S(2)}) collective-permute-start(bf16[512,512]{1,0:T(8,128)(2,1)S(1)} %get-tuple-element.34), channel_id=1, source_target_pairs={{0,3},{1,0},{2,1},{3,2},{4,7},{5,4},{6,5},{7,6},{8,11},{9,8},{10,9... | collective-permute-start | bytes 1572872 | tf_op jit(solution)/shard_map/ppermute | solution.py:28
  141.1 44.5 %collective-permute-start.6 = (bf16[256,1024]{1,0:T(8,128)(2,1)}, bf16[256,1024]{1,0:T(8,128)(2,1)}, u32[]{:S(2)}, u32[]{:S(2)}) collective-permute-start(bf16[256,1024]{1,0:T(8,128)(2,1)} %constant_dynamic-slice_fusion), channel_id=1, source_target_pairs={{0,2},{1,3},{2,0},{3,1},{4,6},{5,7},{6,4},{7,5},{8,10},{9,11},{10,... | collective-permute-start | bytes 1572872 | tf_op jit(solution)/shard_map/ppermute | solution.py:28
  149.2 53.2 %copy-start.6 = (s32[256,2]{0,1:T(2,128)S(1)}, s32[256,2]{0,1:T(2,128)}, u32[]{:S(2)}) copy-start(s32[256,2]{0,1:T(2,128)} %param.22) | copy-start | bytes 6148
  149.2 53.2 %copy-start.7 = (f32[256,2]{0,1:T(2,128)S(1)}, f32[256,2]{0,1:T(2,128)}, u32[]{:S(2)}) copy-start(f32[256,2]{0,1:T(2,128)} %param.23) | copy-start | bytes 6148
  150.3 60.2 %collective-permute-start.7 = (bf16[512,1024]{1,0:T(8,128)(2,1)}, bf16[512,1024]{1,0:T(8,128)(2,1)S(1)}, u32[]{:S(2)}, u32[]{:S(2)}) collective-permute-start(bf16[512,1024]{1,0:T(8,128)(2,1)} %pad_maximum_fusion), channel_id=1, source_target_pairs={{0,4},{4,0},{8,12},{12,8},{16,20},{20,16},{24,28},{28,24},{32,36},... | collective-permute-start | bytes 3145736 | tf_op jit(solution)/shard_map/ppermute | solution.py:38
  169.8 1.0 copy-start.2
  171.8 41.4 %all-to-all-start.1 = ((bf16[64,8,512]{2,1,0:T(8,128)(2,1)}), bf16[64,8,512]{2,1,0:T(8,128)(2,1)}, u32[]{:S(2)}, u32[]{:S(2)}) async-start(bf16[64,8,512]{2,1,0:T(8,128)(2,1)} %bitcast.11), calls=%async_computation.1 | async-start | bytes 1048576 | tf_op jit(solution)/shard_map/all_to_all | solution.py:373
  183.5 13.4 %collective-permute-start = (bf16[32,256]{1,0:T(8,128)(2,1)S(1)}, bf16[32,256]{1,0:T(8,128)(2,1)S(1)}, u32[]{:S(2)}, u32[]{:S(2)}) collective-permute-start(bf16[32,256]{1,0:T(8,128)(2,1)S(1)} %slice.12), channel_id=1, source_target_pairs={{0,4},{4,8},{8,12},{12,16},{16,20},{20,24},{24,28},{28,32},{32,36}... | collective-permute-start | bytes 49160 | tf_op jit(solution)/shard_map/ppermute | solution.py:33
  185.6 24.9 %collective-permute-start.8 = (bf16[256,1024]{1,0:T(8,128)(2,1)}, bf16[256,1024]{1,0:T(8,128)(2,1)}, u32[]{:S(2)}, u32[]{:S(2)}) collective-permute-start(bf16[256,1024]{1,0:T(8,128)(2,1)} %collective-permute-done.6.n3), channel_id=1, source_target_pairs={{0,4},{4,0},{8,12},{12,8},{16,20},{20,16},{24,28},{28,24},{32,36},... | collective-permute-start | bytes 1572872 | tf_op jit(solution)/shard_map/ppermute | solution.py:38
  197.1 6.3 %collective-permute-start.1 = (bf16[256,256]{1,0:T(8,128)(2,1)S(1)}, bf16[256,256]{1,0:T(8,128)(2,1)S(1)}, u32[]{:S(2)}, u32[]{:S(2)}) collective-permute-start(bf16[256,256]{1,0:T(8,128)(2,1)S(1)} %get-tuple-element.53), channel_id=1, source_target_pairs={{0,3},{1,0},{2,1},{3,2},{4,7},{5,4},{6,5},{7,6},{8,11},{9,8},{10,9... | collective-permute-start | bytes 393224 | tf_op jit(solution)/shard_map/ppermute | solution.py:28
  200.8 7.6 %collective-permute-start.2 = (bf16[256,256]{1,0:T(8,128)(2,1)S(1)}, bf16[256,256]{1,0:T(8,128)(2,1)S(1)}, u32[]{:S(2)}, u32[]{:S(2)}) collective-permute-start(bf16[256,256]{1,0:T(8,128)(2,1)S(1)} %get-tuple-element.54), channel_id=1, source_target_pairs={{0,1},{1,2},{2,3},{3,0},{4,5},{5,6},{6,7},{7,4},{8,9},{9,10},{10,1... | collective-permute-start | bytes 393224 | tf_op jit(solution)/shard_map/ppermute | solution.py:28
  200.9 7.6 %collective-permute-start.3 = (bf16[256,256]{1,0:T(8,128)(2,1)S(1)}, bf16[256,256]{1,0:T(8,128)(2,1)S(1)}, u32[]{:S(2)}, u32[]{:S(2)}) collective-permute-start(bf16[256,256]{1,0:T(8,128)(2,1)S(1)} %get-tuple-element.52), channel_id=1, source_target_pairs={{0,2},{1,3},{2,0},{3,1},{4,6},{5,7},{6,4},{7,5},{8,10},{9,11},{10,... | collective-permute-start | bytes 393224 | tf_op jit(solution)/shard_map/ppermute | solution.py:28
  203.0 7.5 %copy-start.4 = (bf16[256,1024]{1,0:T(8,128)(2,1)}, bf16[256,1024]{1,0:T(8,128)(2,1)S(1)}, u32[]{:S(2)}) copy-start(bf16[256,1024]{1,0:T(8,128)(2,1)S(1)} %get-tuple-element.25.high_hbm) | copy-start | bytes 1572868
  203.0 7.5 %copy-start.5 = (bf16[256,1024]{1,0:T(8,128)(2,1)}, bf16[256,1024]{1,0:T(8,128)(2,1)S(1)}, u32[]{:S(2)}) copy-start(bf16[256,1024]{1,0:T(8,128)(2,1)S(1)} %get-tuple-element.26.low_hbm) | copy-start | bytes 1572868

commit v3 on v2

--- a/solution.py
+++ b/solution.py
@@ -36,10 +36,6 @@
 def swap_cores(value):
     count = lax.axis_size("ep")
     return lax.ppermute(value, "ep", [(i, i ^ 1) for i in range(count)])
-
-
-def gather_direct(value):
-    return over_tp(value, -1), over_tp(value, 1), over_tp(value, 2)
 
 
 def gather_relayed(value):
@@ -171,9 +167,9 @@
 
 def second_expert_kernel(
     tp_ref, own, ahead, behind, top, bottom, gate_ref, up_ref, down_ref,
-    to_own, ahead_top, ahead_bottom, behind_top, behind_bottom, across_top, across_bottom,
-    across, to_ahead, to_behind,
+    to_own, to_ahead, to_behind, to_across, across,
 ):
+
     rows, part = own.shape
     half = rows // 2
     across[:half, :] = top[...]
@@ -183,18 +179,11 @@
 
     def step(i, carry):
         at = pl.ds(pl.multiple_of(i * half, half), half)
-        outs = (to_own, to_ahead, to_behind, across)
+        outs = (to_own, to_ahead, to_behind, to_across)
         expert_rows(at, blocks, starts, gate_ref, up_ref, down_ref, outs, lambda k: None)
         return carry
 
     lax.fori_loop(0, 2, step, 0)
-    for source, upper, lower in (
-        (across, across_top, across_bottom),
-        (to_ahead, ahead_top, ahead_bottom),
-        (to_behind, behind_top, behind_bottom),
-    ):
-        upper[...] = source[:half, :]
-        lower[...] = source[half:, :]
 
 
 def fold_kernel(ahead, top, behind, bottom, ahead_out, behind_out):
@@ -210,19 +199,14 @@
     out[...] = sum(term[...].astype(f32) for term in refs[:-1]).astype(bf16)
 
 
-def total_halves_kernel(own, top0, top1, bottom0, bottom1, out, *scratch):
-    half = top0.shape[0]
-    copies = fetch((own, top0, bottom0, top1, bottom1), scratch[:5], scratch[5])
-    for copy in copies:
+def total_fetched_kernel(h0, h1, h2, h3, out, v0, v1, v2, v3, sems):
+    total = None
+    values = (v0, v1, v2, v3)
+    for copy, value in zip(fetch((h0, h1, h2, h3), values, sems), values):
         copy.wait()
-    own, top0, bottom0, top1, bottom1 = (ref[...].astype(f32) for ref in scratch[:5])
-    out[:half, :] = (own[:half, :] + top0 + top1).astype(bf16)
-    out[half:, :] = (own[half:, :] + bottom0 + bottom1).astype(bf16)
-
-
-def fold_halves_kernel(a, b, c, d, ab, cd):
-    ab[...] = (a[...].astype(f32) + b[...].astype(f32)).astype(bf16)
-    cd[...] = (c[...].astype(f32) + d[...].astype(f32)).astype(bf16)
+        term = value[...].astype(f32)
+        total = term if total is None else total + term
+    out[...] = total.astype(bf16)
 
 
 def conv_kernel_body(reach, halo, b0, b1, b2, b3, out_ref, wide, kept):
@@ -257,17 +241,18 @@
         out_ref[:, lanes] = jax.nn.silu(scaled).astype(bf16)
 
 
-def mix_kernel(core_ref, act, own, n1, n2, n3, f12, f3, out_ref):
+def mix_kernel(core_ref, act, own, n1, n2, n3, n4, far_ref, out_ref):
     part = own.shape[0]
     columns = n1.shape[1]
     core = core_ref[0]
     near_at = pl.ds(pl.multiple_of(core * columns, columns), columns)
     far_at = pl.ds(pl.multiple_of((1 - core) * columns, columns), columns)
     cut = lambda k, n=1: act[:, k * part : (k + n) * part]
-    near = dot(cut(0), own[:, near_at]) + dot(cut(1), n1[...])
-    near = near + dot(cut(2), n2[...]) + dot(cut(3), n3[...])
+    near = dot(cut(0), own[:, near_at]) + dot(cut(1), n1[...]) + dot(cut(2), n2[...])
+    near = near + dot(act[:, 3 * part : 3 * part + part // 2], n3[...])
+    near = near + dot(act[:, 3 * part + part // 2 :], n4[...])
     out_ref[:, near_at] = near.astype(bf16)
-    far = dot(cut(0), own[:, far_at]) + dot(cut(1, 2), f12[...]) + dot(cut(3), f3[...])
+    far = dot(cut(0), own[:, far_at]) + dot(cut(1, 3), far_ref[...])
     out_ref[:, far_at] = far.astype(bf16)
 
 
@@ -319,9 +304,9 @@
     columns = out_weight.shape[1] // 2
     mine = lax.dynamic_slice_in_dim(out_weight, core * columns, columns, 1)
     near = [over_tp(mine, -1), over_tp(mine, 1)]
-    far = [swap_cores(jnp.concatenate(near, axis=0))]
-    near.append(over_tp(mine, 2))
-    far.append(swap_cores(near[2]))
+    near.append(over_tp(near[0][: part // 2], -1))
+    near.append(over_tp(near[1][part // 2 :], 1))
+    far = swap_cores(jnp.concatenate(near, axis=0))
     taps = jnp.concatenate([conv_kernel, ln_gain[None, :]], axis=0)
     taps = split_three(taps)
     gated = (glu_value.astype(f32) * jax.nn.sigmoid(glu_gate.astype(f32))).astype(bf16)
@@ -352,7 +337,7 @@
         [SMEM] + [VMEM] * 7,
         2 * own * part * count * 2 * columns,
         8,
-    )(core.astype(jnp.int32).reshape(1), activated, out_weight, *near, *far)
+    )(core.astype(jnp.int32).reshape(1), activated, out_weight, *near, far)
 
 
 def expert_half(moe_input, moe_gain, gate_weight, up_weight, down_weight, expert_ids, route_weight):
@@ -402,7 +387,8 @@
         return call(total_kernel, whole, [VMEM] * len(terms), 10**8, 8)(*terms)
 
     arrived = exchange(sent[0])
-    others = gather_direct(arrived)
+    others = [over_tp(arrived, -1), over_tp(arrived, 1)]
+    others.append(over_tp(arrived, 2))
     own, ahead, behind, top, bottom, *weights = call(
         first_expert_kernel,
         [whole] * 3 + [halves] * 2 + [shape(*w.shape) for w in weights],
@@ -420,38 +406,27 @@
     answers = [exchange(answer)]
     arrived = exchange(sent[1])
     others = gather_relayed(arrived)
-    own, ahead0, ahead1, behind0, behind1, across0, across1 = call(
-        second_expert_kernel,
-        [whole] + [halves] * 6,
-        [SMEM] + [VMEM] * 8,
-        flops,
-        16,
-        vmem_blocks * 3,
+    own, ahead, behind, across = call(
+        second_expert_kernel, [whole] * 4, [SMEM] + [VMEM] * 8, flops, 16, vmem_blocks
     )(tp, arrived, *others, *weights)
-    across0 = over_tp(across0, 1)
-    across1 = over_tp(across1, -1)
-    bottom0 = over_tp(ahead1, 1)
-    top0 = over_tp(behind0, -1)
-    ahead0, behind1 = call(
-        fold_halves_kernel, [halves] * 2, [VMEM] * 4, 10**8, 8
-    )(ahead0, across0, behind1, across1)
-    top1 = over_tp(ahead0, 1)
-    bottom1 = over_tp(behind1, -1)
+    ahead = over_tp(ahead, 1)
+    behind = over_tp(behind, -1)
+    across = over_tp(across, 2)
     answer = call(
-        total_halves_kernel,
+        total_fetched_kernel,
         whole,
-        [ANY] * 5,
+        [ANY] * 4,
         10**8,
         56,
-        vmem_blocks + [pltpu.VMEM((half, part), bf16)] * 4 + [pltpu.SemaphoreType.DMA((5,))],
-    )(own, top0, top1, bottom0, bottom1)
+        vmem_blocks * 4 + [pltpu.SemaphoreType.DMA((4,))],
+    )(own, ahead, behind, across)
     answers.append(exchange(answer))
     return call(
         combine_kernel,
         shape(tokens, part),
         [ANY] * 4,
         4 * tokens * rows * part,
-        56,
+        53,
         [pltpu.VMEM((tokens, experts * capacity), bf16)] * 2
         + vmem_blocks * 2
         + [pltpu.SemaphoreType.DMA((4,))],

time: 217 us -> 219 us (level)
  local copies, waits for them, and re-layouts: 3.53 us -> 21.4 us
  waiting for transfers between devices: 91.3 us -> 81 us
  starting transfers between devices: 62 us -> 54.3 us
  Pallas kernels: 27.8 us -> 30.2 us
    unnamed x28 -> x56, local copies, waits for them, and re-layouts: 2.65 us -> 17.6 us
    all_to_all x3, waiting for transfers between devices: 14.3 us -> 0.01 us  [exchange(): moved = lax.all_to_all(value, 'ep', split_axis=0, concat_axis=0, tiled=True)]
    ppermute x23 -> x21, starting transfers between devices: 35.2 us -> 27.7 us  [over_tp(): lax.ppermute(value, 'tp', [(i, (i + by) % count) for i in range(count)])]
    ppermute x1, waiting for transfers between devices: 9.79 us -> 12.3 us  [from_behind(): return lax.ppermute(value, axis, [(i, i + by) for i in range(count - by)])]
    ppermute x23 -> x21, waiting for transfers between devices: 67.3 us -> 68.6 us  [over_tp(): lax.ppermute(value, 'tp', [(i, (i + by) % count) for i in range(count)])]
    pallas_call x3 -> x2, Pallas kernels: 7.86 us -> 8.78 us  [the longest x1 6.36 us: expert_half(): call(second_expert_kernel, [whole] * 4, [SMEM] + [VMEM] * 8, flops, 16, v...]
  transfers between devices with their start and end apart: 29 -> 26, of which waited for: 13 -> 11; matrix products, arithmetic and copies ran while one was open for 2% -> 2% of each run, Pallas kernels for 7% -> 11%
where the time goes in v3:
time: 219 us; the launch traced here: 218 us
  waiting for transfers between devices  81 us (37%)
  starting transfers between devices  54.3 us (25%)
  Pallas kernels  30.2 us (14%)
  blocking collectives  28 us (13%)
  local copies, waits for them, and re-layouts  21.4 us (10%)
    ppermute x21, waiting for transfers between devices, over_tp(): lax.ppermute(value, 'tp', [(i, (i + by) % count) for i in range(count)])  68.6 us
    all_to_all x1, blocking collectives, exchange(): moved = lax.all_to_all(value, 'ep', split_axis=0, concat_axis=0, tiled=True)  28 us
    ppermute x21, starting transfers between devices, over_tp(): lax.ppermute(value, 'tp', [(i, (i + by) % count) for i in range(count)])  27.7 us
    all_to_all x3, starting transfers between devices, exchange(): moved = lax.all_to_all(value, 'ep', split_axis=0, concat_axis=0, tiled=True)  24.4 us
    unnamed x56, local copies, waits for them, and re-layouts  17.6 us
    ppermute x1, waiting for transfers between devices, from_behind(): return lax.ppermute(value, axis, [(i, i + by) for i in range(count - by)])  12.3 us
    pallas_call x1, Pallas kernels, expert_half(): call(first_expert_kernel, [whole] * 3 + [halves] * 2 + [shape(*w.shape) f...  8.18 us
    pallas_call x1, Pallas kernels, expert_half(): call(second_expert_kernel, [whole] * 4, [SMEM] + [VMEM] * 8, flops, 16, v...  6.36 us
  transfers between devices with their start and end apart: 26, of which 11 were waited for; matrix products, arithmetic and copies ran while one was open for 2% of the time, Pallas kernels for 11%

profile of v3, /device:TPU:96, one launch (start us, length us, event | category | flops | bytes accessed | tf_op | source)
XLA Modules:
  0.0 217.8 jit_solution(15811723596024494085)
XLA Ops:
  0.6 2.9 %shard_map.134 = (bf16[512,512]{1,0:T(8,128)(2,1)}, bf16[512,512]{1,0:T(8,128)(2,1)}) custom-call(s32[1]{0:T(128)} %bitcast.4.tp_ref, bf16[256,2048]{1,0:T(8,128)(2,1)} %x_hbm.1, f32[1,2048]{1,0:T(1,128)} %bitcast.27, s32[2,256]{1,0:T(2,128)} %bitcast.21), custom_call_target="tpu_custom_call" | custom-call | flops 268435456 | bytes 1048576 | tf_op jit(solution)/shard_map/pallas_call | solution.py:361
  3.6 28.0 %all_to_all.20 = bf16[64,8,512]{2,1,0:T(8,128)(2,1)S(1)} all-to-all(bf16[64,8,512]{2,1,0:T(8,128)(2,1)} %bitcast.26), channel_id=1, replica_groups=mesh['ep'=64,'tp'=4] {'ep'}, dimensions={0} | all-to-all | bytes 1048576 | tf_op jit(solution)/shard_map/all_to_all | solution.py:358
  31.6 2.8 %collective-permute-start.9 = (bf16[512,512]{1,0:T(8,128)(2,1)S(1)}, bf16[512,512]{1,0:T(8,128)(2,1)S(1)}, u32[]{:S(2)}, u32[]{:S(2)}) collective-permute-start(bf16[512,512]{1,0:T(8,128)(2,1)S(1)} %bitcast.17), channel_id=1, source_target_pairs={{0,3},{1,0},{2,1},{3,2},{4,7},{5,4},{6,5},{7,6},{8,11},{9,8},{10,9... | collective-permute-start | bytes 1572872 | tf_op jit(solution)/shard_map/ppermute | solution.py:28
  34.3 2.3 %collective-permute-start.11 = (bf16[512,512]{1,0:T(8,128)(2,1)S(1)}, bf16[512,512]{1,0:T(8,128)(2,1)}, u32[]{:S(2)}, u32[]{:S(2)}) collective-permute-start(bf16[512,512]{1,0:T(8,128)(2,1)S(1)} %bitcast.19), channel_id=1, source_target_pairs={{0,2},{1,3},{2,0},{3,1},{4,6},{5,7},{6,4},{7,5},{8,10},{9,11},{10,... | collective-permute-start | bytes 1572872 | tf_op jit(solution)/shard_map/ppermute | solution.py:28
  36.6 6.5 %all-to-all-start.2 = ((bf16[64,8,512]{2,1,0:T(8,128)(2,1)}), bf16[64,8,512]{2,1,0:T(8,128)(2,1)}, u32[]{:S(2)}, u32[]{:S(2)}) async-start(bf16[64,8,512]{2,1,0:T(8,128)(2,1)} %bitcast.25), calls=%async_computation.2 | async-start | bytes 1048576 | tf_op jit(solution)/shard_map/all_to_all | solution.py:358
  43.1 0.8 constant_dynamic-slice_fusion
  44.0 1.1 collective-permute-start.4
  45.1 11.8 %collective-permute-done.9.x1 = bf16[512,512]{1,0:T(8,128)(2,1)S(1)} collective-permute-done((bf16[512,512]{1,0:T(8,128)(2,1)S(1)}, bf16[512,512]{1,0:T(8,128)(2,1)S(1)}, u32[]{:S(2)}, u32[]{:S(2)}) %collective-permute-start.9) | collective-permute-done | bytes 524320 | tf_op jit(solution)/shard_map/ppermute | solution.py:28
  57.7 1.6 collective-permute-done.10.x2
  60.1 1.0 copy-done.11
  61.1 1.0 copy-done.13
  62.2 8.2 %shard_map.135 = (bf16[512,512]{1,0:T(8,128)(2,1)S(1)}, bf16[512,512]{1,0:T(8,128)(2,1)S(1)}, bf16[512,512]{1,0:T(8,128)(2,1)S(1)}, bf16[256,512]{1,0:T(8,128)(2...) custom-call(s32[1]{0:T(128)} %bitcast.4.tp_ref, ...), custom_call_target="tpu_custom_call" | custom-call | flops 4831838208 | bytes 1048576 | tf_op jit(solution)/shard_map/pallas_call | solution.py:392
  71.2 1.6 copy-done.15
  72.8 1.7 copy-done.17
  74.5 1.7 copy-done.19
  76.3 3.1 %collective-permute-start.13 = (bf16[256,512]{1,0:T(8,128)(2,1)}, bf16[256,512]{1,0:T(8,128)(2,1)}, u32[]{:S(2)}, u32[]{:S(2)}) collective-permute-start(bf16[256,512]{1,0:T(8,128)(2,1)} %get-tuple-element.27), channel_id=1, source_target_pairs={{0,3},{1,0},{2,1},{3,2},{4,7},{5,4},{6,5},{7,6},{8,11},{9,8},{10,9... | collective-permute-start | bytes 786440 | tf_op jit(solution)/shard_map/ppermute | solution.py:28
  79.4 3.2 %collective-permute-start.16 = (bf16[512,512]{1,0:T(8,128)(2,1)}, bf16[512,512]{1,0:T(8,128)(2,1)S(1)}, u32[]{:S(2)}, u32[]{:S(2)}) collective-permute-start(bf16[512,512]{1,0:T(8,128)(2,1)} %bitcast.14.own), channel_id=1, source_target_pairs={{0,3},{1,0},{2,1},{3,2},{4,7},{5,4},{6,5},{7,6},{8,11},{9,8},{10,9... | collective-permute-start | bytes 1572872 | tf_op jit(solution)/shard_map/ppermute | solution.py:28
  82.6 4.1 %collective-permute-done.12.top = bf16[256,512]{1,0:T(8,128)(2,1)S(1)} collective-permute-done((bf16[256,512]{1,0:T(8,128)(2,1)}, bf16[256,512]{1,0:T(8,128)(2,1)S(1)}, u32[]{:S(2)}, u32[]{:S(2)}) %collective-permute-start.12) | collective-permute-done | bytes 262176 | tf_op jit(solution)/shard_map/ppermute | solution.py:28
  86.8 1.1 shard_map.136
  88.5 2.9 %collective-permute-start.15 = (bf16[512,512]{1,0:T(8,128)(2,1)S(1)}, bf16[512,512]{1,0:T(8,128)(2,1)S(1)}, u32[]{:S(2)}, u32[]{:S(2)}) collective-permute-start(bf16[512,512]{1,0:T(8,128)(2,1)S(1)} %get-tuple-element.29), channel_id=1, source_target_pairs={{0,3},{1,0},{2,1},{3,2},{4,7},{5,4},{6,5},{7,6},{8,11},{9,8},{10,9... | collective-permute-start | bytes 1572872 | tf_op jit(solution)/shard_map/ppermute | solution.py:28
  92.1 5.9 %collective-permute-done.5.n2 = bf16[256,1024]{1,0:T(8,128)(2,1)S(1)} collective-permute-done((bf16[256,1024]{1,0:T(8,128)(2,1)}, bf16[256,1024]{1,0:T(8,128)(2,1)S(1)}, u32[]{:S(2)}, u32[]{:S(2)}) %collective-permute-start.5) | collective-permute-done | bytes 524320 | tf_op jit(solution)/shard_map/ppermute | solution.py:28
  98.0 1.1 collective-permute-start.6
  99.8 1.0 collective-permute-start.7
  101.5 7.7 %collective-permute-done.17.behind = bf16[512,512]{1,0:T(8,128)(2,1)S(1)} collective-permute-done((bf16[512,512]{1,0:T(8,128)(2,1)}, bf16[512,512]{1,0:T(8,128)(2,1)S(1)}, u32[]{:S(2)}, u32[]{:S(2)}) %collective-permute-start.17) | collective-permute-done | bytes 524320 | tf_op jit(solution)/shard_map/ppermute | solution.py:28
  109.2 1.1 collective-permute-start.18
  111.0 9.4 %collective-permute-done.14.refs_1_ = bf16[512,512]{1,0:T(8,128)(2,1)S(1)} collective-permute-done((bf16[512,512]{1,0:T(8,128)(2,1)S(1)}, bf16[512,512]{1,0:T(8,128)(2,1)S(1)}, u32[]{:S(2)}, u32[]{:S(2)}) %collective-permute-start.14) | collective-permute-done | bytes 524320 | tf_op jit(solution)/shard_map/ppermute | solution.py:28
  120.5 1.0 shard_map.137
  121.5 7.4 %all-to-all-start.1 = ((bf16[64,8,512]{2,1,0:T(8,128)(2,1)}), bf16[64,8,512]{2,1,0:T(8,128)(2,1)}, u32[]{:S(2)}, u32[]{:S(2)}) async-start(bf16[64,8,512]{2,1,0:T(8,128)(2,1)} %bitcast.11), calls=%async_computation.1 | async-start | bytes 1048576 | tf_op jit(solution)/shard_map/all_to_all | solution.py:358
  129.0 1.3 pad_maximum_fusion
  130.5 1.9 copy-done.16
  132.3 1.9 copy-done.18
  134.2 1.9 copy-done.20
  136.1 6.4 %shard_map.138 = (bf16[512,512]{1,0:T(8,128)(2,1)S(1)}, bf16[512,512]{1,0:T(8,128)(2,1)S(1)}, bf16[512,512]{1,0:T(8,128)(2,1)S(1)}, bf16[512,512]{1,0:T(8,128)(2,1)S(1)}) custom-call(s32[1]{0:T(128)} %bitcast.4.tp_ref, bf16[512,512]{1,0:T(8,128)(2,1)} %bitcast.14.own, bf16[512,512]{1,0:T(8,128)(2,1)S(1)} %copy-done.6, bf16[512,512]{1,0:T(8,128)(2,1)S(1)} %copy-done.8, ...), custom_call_target="tpu_custom_call" | custom-call | flops 4831838208 | bytes 1048576 | tf_op jit(solution)/shard_map/pallas_call | solution.py:409
  143.4 3.3 %collective-permute-start.21 = (bf16[512,512]{1,0:T(8,128)(2,1)S(1)}, bf16[512,512]{1,0:T(8,128)(2,1)S(1)}, u32[]{:S(2)}, u32[]{:S(2)}) collective-permute-start(bf16[512,512]{1,0:T(8,128)(2,1)S(1)} %get-tuple-element.36), channel_id=1, source_target_pairs={{0,3},{1,0},{2,1},{3,2},{4,7},{5,4},{6,5},{7,6},{8,11},{9,8},{10,9... | collective-permute-start | bytes 1572872 | tf_op jit(solution)/shard_map/ppermute | solution.py:28
  146.8 1.4 collective-permute-start.22
  148.1 11.0 %collective-permute-done.20.h1 = bf16[512,512]{1,0:T(8,128)(2,1)S(1)} collective-permute-done((bf16[512,512]{1,0:T(8,128)(2,1)S(1)}, bf16[512,512]{1,0:T(8,128)(2,1)S(1)}, u32[]{:S(2)}, u32[]{:S(2)}) %collective-permute-start.20) | collective-permute-done | bytes 524320 | tf_op jit(solution)/shard_map/ppermute | solution.py:28
  159.1 10.6 %collective-permute-done.21.h2 = bf16[512,512]{1,0:T(8,128)(2,1)S(1)} collective-permute-done((bf16[512,512]{1,0:T(8,128)(2,1)S(1)}, bf16[512,512]{1,0:T(8,128)(2,1)S(1)}, u32[]{:S(2)}, u32[]{:S(2)}) %collective-permute-start.21) | collective-permute-done | bytes 524320 | tf_op jit(solution)/shard_map/ppermute | solution.py:28
  169.7 1.8 collective-permute-done.22.h3
  172.4 2.4 %shard_map.139 = bf16[512,512]{1,0:T(8,128)(2,1)} custom-call(bf16[512,512]{1,0:T(8,128)(2,1)} %copy-done.1, bf16[512,512]{1,0:T(8,128)(2,1)} %copy-done.21, bf16[512,512]{1,0:T(8,128)(2,1)} %copy-done.22, bf16[512,512]{1,0:T(8,128)(2,1)} %copy-done.23), custom_call_target="tpu_custom_call" | custom-call | flops 100000000 | bytes 1048576 | tf_op jit(solution)/shard_map/pallas_call | solution.py:415
  174.8 10.5 %all-to-all-start.3 = ((bf16[64,8,512]{2,1,0:T(8,128)(2,1)}), bf16[64,8,512]{2,1,0:T(8,128)(2,1)}, u32[]{:S(2)}, u32[]{:S(2)}) async-start(bf16[64,8,512]{2,1,0:T(8,128)(2,1)} %bitcast.24), calls=%async_computation.3 | async-start | bytes 1048576 | tf_op jit(solution)/shard_map/all_to_all | solution.py:358
  185.5 2.0 collective-permute-start
  187.6 12.3 %collective-permute-done = bf16[32,256]{1,0:T(8,128)(2,1)S(1)} collective-permute-done((bf16[32,256]{1,0:T(8,128)(2,1)S(1)}, bf16[32,256]{1,0:T(8,128)(2,1)S(1)}, u32[]{:S(2)}, u32[]{:S(2)}) %collective-permute-start) | collective-permute-done | bytes 16416 | tf_op jit(solution)/shard_map/ppermute | solution.py:33
  200.1 2.1 collective-permute-start.1
  202.2 1.6 collective-permute-start.3
  205.2 4.7 %collective-permute-done.2.b2 = bf16[256,256]{1,0:T(8,128)(2,1)S(1)} collective-permute-done((bf16[256,256]{1,0:T(8,128)(2,1)S(1)}, bf16[256,256]{1,0:T(8,128)(2,1)S(1)}, u32[]{:S(2)}, u32[]{:S(2)}) %collective-permute-start.2) | collective-permute-done | bytes 131104 | tf_op jit(solution)/shard_map/ppermute | solution.py:28
  209.8 2.0 shard_map.131.act
  211.9 3.0 %shard_map.132 = bf16[128,2048]{1,0:T(8,128)(2,1)} custom-call(s32[1]{0:T(128)} %bitcast.core_ref, bf16[128,1024]{1,0:T(8,128)(2,1)S(1)} %shard_map.131.act, bf16[256,2048]{1,0:T(8,128)(2,1)S(1)} %copy-done, bf16[256,1024]{1,0:T(8,128)(2,1)S(1)} %collective-permute-done.4.n1, bf16[256,1024]{1,0:T(8,128)(2,1)S(1)} %collective-permute-done.5.n2, ...), custom_call_target="tpu_custom_call" | custom-call | flops 536870912 | bytes 1048576 | tf_op jit(solution)/shard_map/pallas_call | solution.py:334
  214.9 2.7 %shard_map.140 = bf16[256,512]{1,0:T(8,128)(2,1)} custom-call(bf16[256,1024]{1,0:T(8,128)(2,1)S(1)} %get-tuple-element.20.high_hbm, bf16[256,1024]{1,0:T(8,128)(2,1)} %copy-done.4, bf16[512,512]{1,0:T(8,128)(2,1)} %bitcast.12.a0_hbm, bf16[512,512]{1,0:T(8,128)(2,1)} %bitcast.16.a1_hbm), custom_call_target="tpu_custom_call" | custom-call | flops 268435456 | bytes 1048576 | tf_op jit(solution)/shard_map/pallas_call | solution.py:424
  (83 shorter events, 9.7 us)
Async XLA Ops:
  0.6 42.5 %copy-start = (bf16[256,2048]{1,0:T(8,128)(2,1)S(1)}, bf16[256,2048]{1,0:T(8,128)(2,1)}, u32[]{:S(2)}) copy-start(bf16[256,2048]{1,0:T(8,128)(2,1)} %own.1) | copy-start | bytes 3145732
  31.6 25.3 %collective-permute-start.9 = (bf16[512,512]{1,0:T(8,128)(2,1)S(1)}, bf16[512,512]{1,0:T(8,128)(2,1)S(1)}, u32[]{:S(2)}, u32[]{:S(2)}) collective-permute-start(bf16[512,512]{1,0:T(8,128)(2,1)S(1)} %bitcast.17), channel_id=1, source_target_pairs={{0,3},{1,0},{2,1},{3,2},{4,7},{5,4},{6,5},{7,6},{8,11},{9,8},{10,9... | collective-permute-start | bytes 1572872 | tf_op jit(solution)/shard_map/ppermute | solution.py:28
  34.3 24.9 %collective-permute-start.10 = (bf16[512,512]{1,0:T(8,128)(2,1)S(1)}, bf16[512,512]{1,0:T(8,128)(2,1)S(1)}, u32[]{:S(2)}, u32[]{:S(2)}) collective-permute-start(bf16[512,512]{1,0:T(8,128)(2,1)S(1)} %bitcast.18), channel_id=1, source_target_pairs={{0,1},{1,2},{2,3},{3,0},{4,5},{5,6},{6,7},{7,4},{8,9},{9,10},{10,1... | collective-permute-start | bytes 1572872 | tf_op jit(solution)/shard_map/ppermute | solution.py:28
  34.3 25.7 %collective-permute-start.11 = (bf16[512,512]{1,0:T(8,128)(2,1)S(1)}, bf16[512,512]{1,0:T(8,128)(2,1)}, u32[]{:S(2)}, u32[]{:S(2)}) collective-permute-start(bf16[512,512]{1,0:T(8,128)(2,1)S(1)} %bitcast.19), channel_id=1, source_target_pairs={{0,2},{1,3},{2,0},{3,1},{4,6},{5,7},{6,4},{7,5},{8,10},{9,11},{10,... | collective-permute-start | bytes 1572872 | tf_op jit(solution)/shard_map/ppermute | solution.py:28
  36.6 42.8 %all-to-all-start.2 = ((bf16[64,8,512]{2,1,0:T(8,128)(2,1)}), bf16[64,8,512]{2,1,0:T(8,128)(2,1)}, u32[]{:S(2)}, u32[]{:S(2)}) async-start(bf16[64,8,512]{2,1,0:T(8,128)(2,1)} %bitcast.25), calls=%async_computation.2 | async-start | bytes 1048576 | tf_op jit(solution)/shard_map/all_to_all | solution.py:358
  44.0 44.5 %collective-permute-start.4 = (bf16[256,1024]{1,0:T(8,128)(2,1)}, bf16[256,1024]{1,0:T(8,128)(2,1)S(1)}, u32[]{:S(2)}, u32[]{:S(2)}) collective-permute-start(bf16[256,1024]{1,0:T(8,128)(2,1)} %constant_dynamic-slice_fusion), channel_id=1, source_target_pairs={{0,3},{1,0},{2,1},{3,2},{4,7},{5,4},{6,5},{7,6},{8,11},{9,8},{10,9... | collective-permute-start | bytes 1572872 | tf_op jit(solution)/shard_map/ppermute | solution.py:28
  60.1 1.0 copy-start.11
  61.1 1.0 copy-start.13
  71.2 1.6 copy-start.15
  72.8 1.7 copy-start.17
  74.4 1.7 copy-start.19
  76.2 10.6 %collective-permute-start.12 = (bf16[256,512]{1,0:T(8,128)(2,1)}, bf16[256,512]{1,0:T(8,128)(2,1)S(1)}, u32[]{:S(2)}, u32[]{:S(2)}) collective-permute-start(bf16[256,512]{1,0:T(8,128)(2,1)} %get-tuple-element.25), channel_id=1, source_target_pairs={{0,1},{1,2},{2,3},{3,0},{4,5},{5,6},{6,7},{7,4},{8,9},{9,10},{10,1... | collective-permute-start | bytes 786440 | tf_op jit(solution)/shard_map/ppermute | solution.py:28
  76.3 10.5 %collective-permute-start.13 = (bf16[256,512]{1,0:T(8,128)(2,1)}, bf16[256,512]{1,0:T(8,128)(2,1)}, u32[]{:S(2)}, u32[]{:S(2)}) collective-permute-start(bf16[256,512]{1,0:T(8,128)(2,1)} %get-tuple-element.27), channel_id=1, source_target_pairs={{0,3},{1,0},{2,1},{3,2},{4,7},{5,4},{6,5},{7,6},{8,11},{9,8},{10,9... | collective-permute-start | bytes 786440 | tf_op jit(solution)/shard_map/ppermute | solution.py:28
  79.4 18.6 %collective-permute-start.5 = (bf16[256,1024]{1,0:T(8,128)(2,1)}, bf16[256,1024]{1,0:T(8,128)(2,1)S(1)}, u32[]{:S(2)}, u32[]{:S(2)}) collective-permute-start(bf16[256,1024]{1,0:T(8,128)(2,1)} %constant_dynamic-slice_fusion), channel_id=1, source_target_pairs={{0,1},{1,2},{2,3},{3,0},{4,5},{5,6},{6,7},{7,4},{8,9},{9,10},{10,1... | collective-permute-start | bytes 1572872 | tf_op jit(solution)/shard_map/ppermute | solution.py:28
  79.4 41.1 %copy-start.3 = (bf16[512,512]{1,0:T(8,128)(2,1)S(1)}, bf16[512,512]{1,0:T(8,128)(2,1)}, u32[]{:S(2)}) copy-start(bf16[512,512]{1,0:T(8,128)(2,1)} %copy-done.2) | copy-start | bytes 1572868
  79.4 20.4 %collective-permute-start.16 = (bf16[512,512]{1,0:T(8,128)(2,1)}, bf16[512,512]{1,0:T(8,128)(2,1)S(1)}, u32[]{:S(2)}, u32[]{:S(2)}) collective-permute-start(bf16[512,512]{1,0:T(8,128)(2,1)} %bitcast.14.own), channel_id=1, source_target_pairs={{0,3},{1,0},{2,1},{3,2},{4,7},{5,4},{6,5},{7,6},{8,11},{9,8},{10,9... | collective-permute-start | bytes 1572872 | tf_op jit(solution)/shard_map/ppermute | solution.py:28
  86.8 22.5 %collective-permute-start.17 = (bf16[512,512]{1,0:T(8,128)(2,1)}, bf16[512,512]{1,0:T(8,128)(2,1)S(1)}, u32[]{:S(2)}, u32[]{:S(2)}) collective-permute-start(bf16[512,512]{1,0:T(8,128)(2,1)} %bitcast.14.own), channel_id=1, source_target_pairs={{0,1},{1,2},{2,3},{3,0},{4,5},{5,6},{6,7},{7,4},{8,9},{9,10},{10,1... | collective-permute-start | bytes 1572872 | tf_op jit(solution)/shard_map/ppermute | solution.py:28
  87.9 32.6 %collective-permute-start.14 = (bf16[512,512]{1,0:T(8,128)(2,1)S(1)}, bf16[512,512]{1,0:T(8,128)(2,1)S(1)}, u32[]{:S(2)}, u32[]{:S(2)}) collective-permute-start(bf16[512,512]{1,0:T(8,128)(2,1)S(1)} %get-tuple-element.28), channel_id=1, source_target_pairs={{0,1},{1,2},{2,3},{3,0},{4,5},{5,6},{6,7},{7,4},{8,9},{9,10},{10,1... | collective-permute-start | bytes 1572872 | tf_op jit(solution)/shard_map/ppermute | solution.py:28
  88.5 32.0 %collective-permute-start.15 = (bf16[512,512]{1,0:T(8,128)(2,1)S(1)}, bf16[512,512]{1,0:T(8,128)(2,1)S(1)}, u32[]{:S(2)}, u32[]{:S(2)}) collective-permute-start(bf16[512,512]{1,0:T(8,128)(2,1)S(1)} %get-tuple-element.29), channel_id=1, source_target_pairs={{0,3},{1,0},{2,1},{3,2},{4,7},{5,4},{6,5},{7,6},{8,11},{9,8},{10,9... | collective-permute-start | bytes 1572872 | tf_op jit(solution)/shard_map/ppermute | solution.py:28
  98.0 30.9 %collective-permute-start.6 = (bf16[128,1024]{1,0:T(8,128)(2,1)}, bf16[128,1024]{1,0:T(8,128)(2,1)S(1)}, u32[]{:S(2)}, u32[]{:S(2)}) collective-permute-start(bf16[128,1024]{1,0:T(8,128)(2,1)} %slice.21), channel_id=1, source_target_pairs={{0,3},{1,0},{2,1},{3,2},{4,7},{5,4},{6,5},{7,6},{8,11},{9,8},{10,9... | collective-permute-start | bytes 786440 | tf_op jit(solution)/shard_map/ppermute | solution.py:28
  99.8 21.7 %copy-start.5 = (bf16[512,512]{1,0:T(8,128)(2,1)}, bf16[512,512]{1,0:T(8,128)(2,1)S(1)}, u32[]{:S(2)}) copy-start(bf16[512,512]{1,0:T(8,128)(2,1)S(1)} %collective-permute-done.16.ahead) | copy-start | bytes 1572868
  99.8 29.1 %collective-permute-start.7 = (bf16[128,1024]{1,0:T(8,128)(2,1)}, bf16[128,1024]{1,0:T(8,128)(2,1)S(1)}, u32[]{:S(2)}, u32[]{:S(2)}) collective-permute-start(bf16[128,1024]{1,0:T(8,128)(2,1)} %slice.22), channel_id=1, source_target_pairs={{0,1},{1,2},{2,3},{3,0},{4,5},{5,6},{6,7},{7,4},{8,9},{9,10},{10,1... | collective-permute-start | bytes 786440 | tf_op jit(solution)/shard_map/ppermute | solution.py:28
  109.2 12.2 %copy-start.7 = (bf16[512,512]{1,0:T(8,128)(2,1)}, bf16[512,512]{1,0:T(8,128)(2,1)S(1)}, u32[]{:S(2)}) copy-start(bf16[512,512]{1,0:T(8,128)(2,1)S(1)} %collective-permute-done.17.behind) | copy-start | bytes 1572868
  109.2 21.2 %collective-permute-start.18 = (bf16[256,512]{1,0:T(8,128)(2,1)}, bf16[256,512]{1,0:T(8,128)(2,1)S(1)}, u32[]{:S(2)}, u32[]{:S(2)}) collective-permute-start(bf16[256,512]{1,0:T(8,128)(2,1)} %slice.23), channel_id=1, source_target_pairs={{0,3},{1,0},{2,1},{3,2},{4,7},{5,4},{6,5},{7,6},{8,11},{9,8},{10,9... | collective-permute-start | bytes 786440 | tf_op jit(solution)/shard_map/ppermute | solution.py:28
  120.5 10.0 %collective-permute-start.19 = (bf16[256,512]{1,0:T(8,128)(2,1)}, bf16[256,512]{1,0:T(8,128)(2,1)}, u32[]{:S(2)}, u32[]{:S(2)}) collective-permute-start(bf16[256,512]{1,0:T(8,128)(2,1)} %slice.24), channel_id=1, source_target_pairs={{0,1},{1,2},{2,3},{3,0},{4,5},{5,6},{6,7},{7,4},{8,9},{9,10},{10,1... | collective-permute-start | bytes 786440 | tf_op jit(solution)/shard_map/ppermute | solution.py:28
  121.5 9.0 %copy-start.6 = (bf16[512,512]{1,0:T(8,128)(2,1)S(1)}, bf16[512,512]{1,0:T(8,128)(2,1)}, u32[]{:S(2)}) copy-start(bf16[512,512]{1,0:T(8,128)(2,1)} %copy-done.5) | copy-start | bytes 1572868
  121.5 53.3 %all-to-all-start.1 = ((bf16[64,8,512]{2,1,0:T(8,128)(2,1)}), bf16[64,8,512]{2,1,0:T(8,128)(2,1)}, u32[]{:S(2)}, u32[]{:S(2)}) async-start(bf16[64,8,512]{2,1,0:T(8,128)(2,1)} %bitcast.11), calls=%async_computation.1 | async-start | bytes 1048576 | tf_op jit(solution)/shard_map/all_to_all | solution.py:358
  128.9 1.5 copy-start.8
  130.3 81.5 %collective-permute-start.8 = (bf16[768,1024]{1,0:T(8,128)(2,1)}, bf16[768,1024]{1,0:T(8,128)(2,1)}, u32[]{:S(2)}, u32[]{:S(2)}) collective-permute-start(bf16[768,1024]{1,0:T(8,128)(2,1)} %pad_maximum_fusion), channel_id=1, source_target_pairs={{0,4},{4,0},{8,12},{12,8},{16,20},{20,16},{24,28},{28,24},{32,36},... | collective-permute-start | bytes 4718600 | tf_op jit(solution)/shard_map/ppermute | solution.py:38
  130.4 1.9 copy-start.16
  132.3 1.9 copy-start.18
  134.2 1.9 copy-start.20
  143.3 42.0 %copy-start.24 = (bf16[512,256]{1,0:T(8,128)(2,1)S(1)}, bf16[512,256]{1,0:T(8,128)(2,1)}, u32[]{:S(2)}) copy-start(bf16[512,256]{1,0:T(8,128)(2,1)} %param.13) | copy-start | bytes 786436
  143.3 42.0 %copy-start.25 = (bf16[512,256]{1,0:T(8,128)(2,1)S(1)}, bf16[512,256]{1,0:T(8,128)(2,1)}, u32[]{:S(2)}) copy-start(bf16[512,256]{1,0:T(8,128)(2,1)} %param.12) | copy-start | bytes 786436
  143.3 44.2 %copy-start.26 = (f32[31,256]{1,0:T(8,128)S(1)}, f32[31,256]{1,0:T(8,128)}, u32[]{:S(2)}) copy-start(f32[31,256]{1,0:T(8,128)} %param.14) | copy-start | bytes 95236
  143.3 44.2 %copy-start.27 = (f32[256]{0:T(256)S(1)}, f32[256]{0:T(256)}, u32[]{:S(2)}) copy-start(f32[256]{0:T(256)} %param.15) | copy-start | bytes 3076
  143.3 60.5 %copy-start.9 = (s32[256,2]{0,1:T(2,128)S(1)}, s32[256,2]{0,1:T(2,128)}, u32[]{:S(2)}) copy-start(s32[256,2]{0,1:T(2,128)} %param.22) | copy-start | bytes 6148
  143.3 60.5 %copy-start.14 = (f32[256,2]{0,1:T(2,128)S(1)}, f32[256,2]{0,1:T(2,128)}, u32[]{:S(2)}) copy-start(f32[256,2]{0,1:T(2,128)} %param.23) | copy-start | bytes 6148
  143.3 15.8 %collective-permute-start.20 = (bf16[512,512]{1,0:T(8,128)(2,1)S(1)}, bf16[512,512]{1,0:T(8,128)(2,1)S(1)}, u32[]{:S(2)}, u32[]{:S(2)}) collective-permute-start(bf16[512,512]{1,0:T(8,128)(2,1)S(1)} %get-tuple-element.35), channel_id=1, source_target_pairs={{0,1},{1,2},{2,3},{3,0},{4,5},{5,6},{6,7},{7,4},{8,9},{9,10},{10,1... | collective-permute-start | bytes 1572872 | tf_op jit(solution)/shard_map/ppermute | solution.py:28
  143.4 26.3 %collective-permute-start.21 = (bf16[512,512]{1,0:T(8,128)(2,1)S(1)}, bf16[512,512]{1,0:T(8,128)(2,1)S(1)}, u32[]{:S(2)}, u32[]{:S(2)}) collective-permute-start(bf16[512,512]{1,0:T(8,128)(2,1)S(1)} %get-tuple-element.36), channel_id=1, source_target_pairs={{0,3},{1,0},{2,1},{3,2},{4,7},{5,4},{6,5},{7,6},{8,11},{9,8},{10,9... | collective-permute-start | bytes 1572872 | tf_op jit(solution)/shard_map/ppermute | solution.py:28
  146.8 24.8 %collective-permute-start.22 = (bf16[512,512]{1,0:T(8,128)(2,1)S(1)}, bf16[512,512]{1,0:T(8,128)(2,1)S(1)}, u32[]{:S(2)}, u32[]{:S(2)}) collective-permute-start(bf16[512,512]{1,0:T(8,128)(2,1)S(1)} %get-tuple-element.37), channel_id=1, source_target_pairs={{0,2},{1,3},{2,0},{3,1},{4,6},{5,7},{6,4},{7,5},{8,10},{9,11},{10,... | collective-permute-start | bytes 1572872 | tf_op jit(solution)/shard_map/ppermute | solution.py:28
  159.1 12.4 %copy-start.21 = (bf16[512,512]{1,0:T(8,128)(2,1)}, bf16[512,512]{1,0:T(8,128)(2,1)S(1)}, u32[]{:S(2)}) copy-start(bf16[512,512]{1,0:T(8,128)(2,1)S(1)} %collective-permute-done.20.h1) | copy-start | bytes 1572868
  169.7 1.8 copy-start.22
  174.8 40.1 %all-to-all-start.3 = ((bf16[64,8,512]{2,1,0:T(8,128)(2,1)}), bf16[64,8,512]{2,1,0:T(8,128)(2,1)}, u32[]{:S(2)}, u32[]{:S(2)}) async-start(bf16[64,8,512]{2,1,0:T(8,128)(2,1)} %bitcast.24), calls=%async_computation.3 | async-start | bytes 1048576 | tf_op jit(solution)/shard_map/all_to_all | solution.py:358
  185.5 14.5 %collective-permute-start = (bf16[32,256]{1,0:T(8,128)(2,1)S(1)}, bf16[32,256]{1,0:T(8,128)(2,1)S(1)}, u32[]{:S(2)}, u32[]{:S(2)}) collective-permute-start(bf16[32,256]{1,0:T(8,128)(2,1)S(1)} %slice.20), channel_id=1, source_target_pairs={{0,4},{4,8},{8,12},{12,16},{16,20},{20,24},{24,28},{28,32},{32,36}... | collective-permute-start | bytes 49160 | tf_op jit(solution)/shard_map/ppermute | solution.py:33
  200.1 5.1 %collective-permute-start.1 = (bf16[256,256]{1,0:T(8,128)(2,1)S(1)}, bf16[256,256]{1,0:T(8,128)(2,1)S(1)}, u32[]{:S(2)}, u32[]{:S(2)}) collective-permute-start(bf16[256,256]{1,0:T(8,128)(2,1)S(1)} %get-tuple-element.43), channel_id=1, source_target_pairs={{0,3},{1,0},{2,1},{3,2},{4,7},{5,4},{6,5},{7,6},{8,11},{9,8},{10,9... | collective-permute-start | bytes 393224 | tf_op jit(solution)/shard_map/ppermute | solution.py:28
  202.2 7.6 %collective-permute-start.2 = (bf16[256,256]{1,0:T(8,128)(2,1)S(1)}, bf16[256,256]{1,0:T(8,128)(2,1)S(1)}, u32[]{:S(2)}, u32[]{:S(2)}) collective-permute-start(bf16[256,256]{1,0:T(8,128)(2,1)S(1)} %get-tuple-element.44), channel_id=1, source_target_pairs={{0,1},{1,2},{2,3},{3,0},{4,5},{5,6},{6,7},{7,4},{8,9},{9,10},{10,1... | collective-permute-start | bytes 393224 | tf_op jit(solution)/shard_map/ppermute | solution.py:28
  202.2 7.6 %collective-permute-start.3 = (bf16[256,256]{1,0:T(8,128)(2,1)S(1)}, bf16[256,256]{1,0:T(8,128)(2,1)S(1)}, u32[]{:S(2)}, u32[]{:S(2)}) collective-permute-start(bf16[256,256]{1,0:T(8,128)(2,1)S(1)} %get-tuple-element.42), channel_id=1, source_target_pairs={{0,2},{1,3},{2,0},{3,1},{4,6},{5,7},{6,4},{7,5},{8,10},{9,11},{10,... | collective-permute-start | bytes 393224 | tf_op jit(solution)/shard_map/ppermute | solution.py:28
  (6 other events, 4.8 us)
